TPU v7x, 32 devices: a whole 2x2x4 slice. The times are simulated.
32 devices in a mesh: grp: 2 (over x), ep: 16 (over z, y, core).
Axes of the slice: x: 2, y: 2, z: 4, core: 2. Of those that a mesh axis runs over, the one named last changes fastest.
Arguments:
- hidden: bfloat16 [96, 2048], P(('grp', 'ep')), parts along dimension 0, may hold values from -6 to 6
- conv_window: bfloat16 [96, 3, 6144], P(('grp', 'ep')), parts along dimension 0, may hold values from -6 to 6
- ssm_state: float32 [96, 64, 64, 128], P(('grp', 'ep')), parts along dimension 0, may hold values from -1.75 to 1.75
- gate_proj: bfloat16 [2048, 4096], P(None, 'ep'), may hold values from -0.125 to 0.125
- input_proj: bfloat16 [2048, 4096], P(None, 'ep'), may hold values from -0.125 to 0.125
- write_proj: bfloat16 [2048, 1024], P(None, 'ep'), may hold values from -0.125 to 0.125
- read_proj: bfloat16 [2048, 1024], P(None, 'ep'), may hold values from -0.125 to 0.125
- step_proj: bfloat16 [2048, 64], replicated, may hold values from -0.125 to 0.125
- step_bias: float32 [64], replicated, may hold values from -2 to 1
- decay_log: float32 [64], replicated, may hold values from -2.3 to 1.4
- decay_shift: float32 [96, 64], P(('grp', 'ep')), parts along dimension 0, may hold values from -0.7 to 0
- skip_scale: float32 [64], replicated, may hold values from -4 to 4
- conv_taps: bfloat16 [4, 6144], replicated, may hold values from -3 to 3
- conv_bias: float32 [6144], replicated, may hold values from -3 to 3
- mix_gain: float32 [2048], replicated, may hold values from 0.1 to 1.9
- group_gain: float32 [4096], replicated, may hold values from 0.1 to 1.9
- out_proj: bfloat16 [4096, 2048], P(None, 'ep'), may hold values from -0.09375 to 0.09375
- ffn_gain: float32 [2048], replicated, may hold values from 0.1 to 1.9
- router: bfloat16 [2048, 16], replicated, may hold values from -0.125 to 0.125
- expert_ids: int32 [96, 6], P(('grp', 'ep')), parts along dimension 0, may hold values from 0 to 15, all different within a row; in each aligned block of 3 rows (0 to 2, 3 to 5, ...) at most 2 rows name the same one
- expert_gate: bfloat16 [16, 2048, 512], P('ep'), may hold values from -0.125 to 0.125
- expert_up: bfloat16 [16, 2048, 512], P('ep'), may hold values from -0.125 to 0.125
- expert_down: bfloat16 [16, 512, 2048], P('ep'), may hold values from -0.25 to 0.25
- shared_gate: bfloat16 [2048, 512], P('ep'), may hold values from -0.125 to 0.125
- shared_up: bfloat16 [2048, 512], P('ep'), may hold values from -0.125 to 0.125
- shared_down: bfloat16 [512, 2048], replicated, may hold values from -0.25 to 0.25
Outputs:
- layer_out: bfloat16 [96, 2048], P(('grp', 'ep')), parts along dimension 0
- next_state: float32 [96, 64, 64, 128], P(('grp', 'ep')), parts along dimension 0
- next_window: bfloat16 [96, 3, 6144], P(('grp', 'ep')), parts along dimension 0
There are 2 independent parts, one for each index of `grp`. A program takes and returns all parts, laid end to end along the dimension named above; an argument that names none is the same for every part. Nothing has to cross between parts.
Inputs may be any that keep to these rules, and one draw needn't show every extreme that they name: `expert_ids`: each row names 6 different experts; in the rows of one device no expert is named by more than 2 rows, and in every draw some device's rows name some expert exactly 2 times.
All inputs are finite; a program needn't handle non-finite values.
Results may differ from a plain program's by a relative error of at most 0.019.
Values may be sent and summed in bfloat16 or wider, within the bound.
A program may use at most 128 MiB of HBM per device.

v0:
```python
import functools

import jax
import jax.numpy as jnp
from jax import lax
from jax.experimental import pallas as pl
from jax.experimental.pallas import tpu as pltpu
from jax.sharding import PartitionSpec as P

HEAD_DIM = 64
GROUPS = 8
STATE = 128


epsilon = 1e-06
routed_scale = 2.5


def row_scale(values):
    return lax.rsqrt(jnp.mean(values * values, axis=-1, keepdims=True) + epsilon)


def matmul(left, right):
    return jnp.dot(left, right, preferred_element_type=jnp.float32)


def expert_result(rows_in, weight_gate, weight_up, weight_down):
    expert_hidden = (jax.nn.silu(matmul(rows_in, weight_gate)) * matmul(rows_in, weight_up)).astype(
        jnp.bfloat16
    )
    return matmul(expert_hidden, weight_down).astype(jnp.bfloat16)


def exchange_kernel(n, spread, source, landed, send_sem, recv_sem, own_sem):
    me = lax.axis_index("ep")
    barrier = pltpu.get_barrier_semaphore()
    for step in range(1, n):
        pl.semaphore_signal(
            barrier, inc=1, device_id={"ep": lax.rem(me + step, n)}, device_id_type=pl.DeviceIdType.MESH
        )
    own = pltpu.make_async_copy(source if spread else source.at[me], landed.at[me], own_sem)
    own.start()
    pl.semaphore_wait(barrier, n - 1)
    copies = []
    for step in range(1, n):
        target = lax.rem(me + step, n)
        copy = pltpu.make_async_remote_copy(
            src_ref=source if spread else source.at[target],
            dst_ref=landed.at[me],
            send_sem=send_sem.at[step],
            recv_sem=recv_sem.at[step],
            device_id={"ep": target},
            device_id_type=pl.DeviceIdType.MESH,
        )
        copy.start()
        copies.append(copy)
    own.wait()
    for copy in copies:
        copy.wait()


def send(source, shape, spread, ident):
    n = shape[0]
    return pl.pallas_call(
        functools.partial(exchange_kernel, n, spread),
        out_shape=jax.ShapeDtypeStruct(shape, source.dtype),
        in_specs=[pl.BlockSpec(memory_space=pltpu.VMEM)],
        out_specs=pl.BlockSpec(memory_space=pltpu.VMEM),
        scratch_shapes=[
            pltpu.SemaphoreType.DMA((n,)),
            pltpu.SemaphoreType.DMA((n,)),
            pltpu.SemaphoreType.DMA,
        ],
        compiler_params=pltpu.CompilerParams(collective_id=ident, has_side_effects=True),
    )(source)


def exchange(blocks, ident):
    return send(blocks, blocks.shape, False, ident)


def gather(block, ident):
    return send(block, (lax.axis_size("ep"),) + block.shape, True, ident)


def transposed(left, right):
    return lax.dot_general(left, right, (((1,), (1,)), ((), ())), preferred_element_type=jnp.float32)


def state_kernel(per_group, decay, inputs, write, read, carried, updated, mixed):
    row, part = pl.program_id(0), pl.program_id(1)
    heads = carried.shape[1]
    scaled = inputs[0, 0]
    lane = lax.broadcasted_iota(jnp.int32, scaled.shape, 1)
    total = jnp.zeros(scaled.shape, jnp.float32)
    entries = carried.shape[3]
    head_dim = carried.shape[2]
    for group in range(heads // per_group):
        write_row = write[0, 0, group : group + 1]
        spread = jnp.broadcast_to(read[0, 0, group : group + 1], (entries, entries))
        spread_high = spread.astype(jnp.bfloat16)
        spread_low = (spread - spread_high.astype(jnp.float32)).astype(jnp.bfloat16)
        pieces = []
        for head in range(group * per_group, (group + 1) * per_group):
            fresh = (
                carried[0, head] * decay[row, part * heads + head]
                + scaled[:, head : head + 1] * write_row
            )
            updated[0, head] = fresh
            pieces.append(fresh)
        stacked = jnp.concatenate(pieces, axis=0)
        high = stacked.astype(jnp.bfloat16)
        low = (stacked - high.astype(jnp.float32)).astype(jnp.bfloat16)
        columns = transposed(high, spread_high) + transposed(low, spread_high) + transposed(high, spread_low)
        for place in range(per_group):
            head = group * per_group + place
            column = columns[place * head_dim : (place + 1) * head_dim, :heads]
            total = jnp.where(lane == head, column, total)
    mixed[0, 0] = total


def state_step(state, decay_rate, scaled, write_vec, read_vec):
    rows, head_count, head_dim, entries = state.shape
    groups = write_vec.shape[1]
    parts = 2
    heads = head_count // parts
    inputs = scaled.reshape(rows, parts, heads, head_dim).transpose(0, 1, 3, 2)
    vec_shape = (rows, parts, groups // parts, entries)
    part_spec = lambda *dims: pl.BlockSpec((1, 1) + dims, lambda row, part: (row, part, 0, 0))
    state_spec = pl.BlockSpec((1, heads, head_dim, entries), lambda row, part: (row, part, 0, 0))
    next_state, mixed = pl.pallas_call(
        functools.partial(state_kernel, head_count // groups),
        grid=(rows, parts),
        out_shape=(
            jax.ShapeDtypeStruct(state.shape, jnp.float32),
            jax.ShapeDtypeStruct(inputs.shape, jnp.float32),
        ),
        in_specs=[
            pl.BlockSpec(memory_space=pltpu.SMEM),
            part_spec(head_dim, heads),
            part_spec(groups // parts, entries),
            part_spec(groups // parts, entries),
            state_spec,
        ],
        out_specs=(state_spec, part_spec(head_dim, heads)),
    )(decay_rate, inputs, write_vec.reshape(vec_shape), read_vec.reshape(vec_shape), state)
    return next_state, mixed.transpose(0, 1, 3, 2).reshape(rows, head_count, head_dim)


def shards(
    hidden,
    conv_window,
    ssm_state,
    gate_proj,
    input_proj,
    write_proj,
    read_proj,
    step_proj,
    step_bias,
    decay_log,
    decay_shift,
    skip_scale,
    conv_taps,
    conv_bias,
    mix_gain,
    group_gain,
    out_proj,
    ffn_gain,
    router,
    expert_ids,
    expert_gate,
    expert_up,
    expert_down,
    shared_gate,
    shared_up,
    shared_down,
):
    local_rows = hidden.shape[0]
    device_index = lax.axis_index("ep")
    width = hidden.shape[1]
    first_row = device_index * local_rows
    gathered = gather(hidden, 0).reshape(-1, width)
    gathered_wide = gathered.astype(jnp.float32)
    normed = (gathered_wide * row_scale(gathered_wide) * mix_gain).astype(jnp.bfloat16)
    parts = [matmul(normed, proj).astype(jnp.bfloat16) for proj in (gate_proj, input_proj, write_proj, read_proj)]
    outbound = jnp.concatenate(parts, axis=1)
    arrived = exchange(outbound.reshape(-1, local_rows, outbound.shape[1]), 1)
    rows, offset = [], 0
    for part in parts:
        piece = arrived[:, :, offset : offset + part.shape[1]]
        rows.append(piece.transpose(1, 0, 2).reshape(local_rows, -1))
        offset += part.shape[1]
    gate_rows, input_rows, write_rows, read_rows = rows
    hidden_wide = hidden.astype(jnp.float32)
    normed_local = (hidden_wide * row_scale(hidden_wide) * mix_gain).astype(jnp.bfloat16)
    step_raw = matmul(normed_local, step_proj)
    inner_width = gate_rows.shape[1]
    state_span = GROUPS * STATE
    head_count = step_bias.shape[0]
    fresh_row = jnp.concatenate([input_rows, write_rows, read_rows], axis=1)
    window = jnp.concatenate([conv_window, fresh_row[:, None, :]], axis=1)
    convolved = jax.nn.silu(
        jnp.sum(window.astype(jnp.float32) * conv_taps.astype(jnp.float32)[None], axis=1)
        + conv_bias
    )
    head_input = convolved[:, :inner_width].reshape(local_rows, head_count, HEAD_DIM)
    write_vec = convolved[:, inner_width : inner_width + state_span].reshape(
        local_rows, GROUPS, STATE
    )
    read_vec = convolved[:, inner_width + state_span :].reshape(local_rows, GROUPS, STATE)
    step_size = jax.nn.softplus(step_raw + step_bias)
    decay_rate = jnp.exp(decay_shift - step_size * jnp.exp(decay_log))
    next_state, mixed_out = state_step(
        ssm_state, decay_rate, step_size[:, :, None] * head_input, write_vec, read_vec
    )
    mixed_out = mixed_out + skip_scale[None, :, None] * head_input
    mixed_out = mixed_out.reshape(local_rows, inner_width).astype(jnp.bfloat16)
    gated_out = mixed_out.astype(jnp.float32) * jax.nn.silu(gate_rows.astype(jnp.float32))
    blocks = gated_out.reshape(local_rows, GROUPS, -1)
    gated_out = ((blocks * row_scale(blocks)).reshape(local_rows, inner_width) * group_gain).astype(
        jnp.bfloat16
    )
    col_width = out_proj.shape[1]
    resid_cols = lax.dynamic_slice_in_dim(gathered_wide, device_index * col_width, col_width, 1)
    resid_part = (
        resid_cols + matmul(gather(gated_out, 2).reshape(-1, inner_width), out_proj)
    ).astype(jnp.bfloat16)
    resid_all = gather(resid_part, 3).transpose(1, 0, 2).reshape(-1, width)
    gain_part = lax.dynamic_slice_in_dim(ffn_gain, device_index * col_width, col_width, 0)
    shared_part = (resid_part.astype(jnp.float32) * gain_part).astype(jnp.bfloat16)
    shared_pre = jnp.concatenate(
        [matmul(shared_part, shared_gate), matmul(shared_part, shared_up)], axis=1
    ).astype(jnp.bfloat16)
    resid_all_wide = resid_all.astype(jnp.float32)
    scale_all = row_scale(resid_all_wide)
    routed_all = (resid_all_wide * scale_all * ffn_gain).astype(jnp.bfloat16)
    result = expert_result(routed_all, expert_gate[0], expert_up[0], expert_down[0])
    back = exchange(
        jnp.concatenate([result, shared_pre], axis=1).reshape(
            -1, local_rows, width + shared_pre.shape[1]
        ),
        4,
    ).astype(jnp.float32)
    resid_wide = lax.dynamic_slice_in_dim(resid_all_wide, first_row, local_rows, 0)
    norm_scale = lax.dynamic_slice_in_dim(scale_all, first_row, local_rows, 0)
    routed_in = lax.dynamic_slice_in_dim(routed_all, first_row, local_rows, 0)
    scores = jax.nn.sigmoid(matmul(routed_in, router))
    chosen = jnp.any(
        expert_ids[:, :, None] == jnp.arange(router.shape[1], dtype=jnp.int32)[None, None, :], axis=1
    )
    scores = jnp.where(chosen, scores, 0.0)
    weights = routed_scale * scores / jnp.sum(scores, axis=1, keepdims=True)
    routed = jnp.sum(back[:, :, :width] * weights.T[:, :, None], axis=0)
    shared_sum = jnp.sum(back[:, :, width:], axis=0)
    hidden_units = shared_down.shape[0]
    shared_hidden = (
        jax.nn.silu(norm_scale * shared_sum[:, :hidden_units])
        * (norm_scale * shared_sum[:, hidden_units:])
    ).astype(jnp.bfloat16)
    layer_out = (resid_wide + routed + matmul(shared_hidden, shared_down)).astype(jnp.bfloat16)
    return (layer_out, next_state, window[:, 1:])


def solution(mesh):
    placed = (
        P(("grp", "ep"), None),
        P(("grp", "ep"), None, None),
        P(("grp", "ep"), None, None, None),
        P(None, "ep"),
        P(None, "ep"),
        P(None, "ep"),
        P(None, "ep"),
        P(),
        P(),
        P(),
        P(("grp", "ep"), None),
        P(),
        P(),
        P(),
        P(),
        P(),
        P(None, "ep"),
        P(),
        P(),
        P(("grp", "ep"), None),
        P("ep", None, None),
        P("ep", None, None),
        P("ep", None, None),
        P("ep", None),
        P("ep", None),
        P(),
    )
    return jax.shard_map(
        shards,
        mesh=mesh,
        in_specs=placed,
        out_specs=(
            P(("grp", "ep"), None),
            P(("grp", "ep"), None, None, None),
            P(("grp", "ep"), None, None),
        ),
        check_vma=False,
    )
```

profile of v0, /device:TPU:0, one launch (start us, length us, event | category | flops | bytes accessed | tf_op | source)
XLA Modules:
  0.0 107.7 jit_solution(9910501801766522415)
XLA Ops:
  0.7 12.7 %shard_map.265 = bf16[16,3,2048]{2,1,0:T(4,128)(2,1)} custom-call(bf16[3,2048]{1,0:T(4,128)(2,1)} %source.1), custom_call_target="tpu_custom_call" | custom-call | tf_op jit(solution)/shard_map/pallas_call | solution.py:64
  13.4 1.1 %reshape.148 = f32[48,2048]{1,0:T(8,128)S(1)} reshape(bf16[16,3,2048]{2,1,0:T(4,128)(2,1)} %shard_map.265) | data formatting | bytes 589824 | tf_op jit(solution)/shard_map/convert_element_type | solution.py:183
  14.5 1.2 %multiply_reduce_fusion = f32[16,3]{1,0:T(8,128)S(1)} fusion(bf16[16,3,2048]{2,1,0:T(4,128)(2,1)} %shard_map.265), kind=kLoop, calls=%fused_computation.29 | loop fusion | flops 294864 | bytes 196800 | tf_op jit(solution)/shard_map/reduce_sum | solution.py:20
  15.6 0.1 rsqrt.42
  15.7 0.9 multiply_convert_fusion
  16.6 1.2 %convolution_convert_fusion.5 = bf16[48,64]{1,0:T(8,128)(2,1)S(1)} fusion(bf16[48,2048]{1,0:T(8,128)(2,1)S(1)} %multiply_convert_fusion, bf16[2048,64]{0,1:T(8,128)(2,1)} %param.32), kind=kOutput, calls=%fused_computation.16 | convolution fusion | flops 12585984 | bytes 464896 | tf_op jit(solution)/shard_map/dot_general | solution.py:24
  17.8 1.2 %convolution_convert_fusion.6 = bf16[48,64]{1,0:T(8,128)(2,1)S(1)} fusion(bf16[48,2048]{1,0:T(8,128)(2,1)S(1)} %multiply_convert_fusion, bf16[2048,64]{0,1:T(8,128)(2,1)} %param.31), kind=kOutput, calls=%fused_computation.17 | convolution fusion | flops 12585984 | bytes 464896 | tf_op jit(solution)/shard_map/dot_general | solution.py:24
  19.0 0.3 convolution_convert_fusion.3
  19.4 0.3 convolution_convert_fusion.4
  19.7 0.7 reshape.140.source
  20.4 10.0 %shard_map.266 = bf16[16,3,640]{2,1,0:T(4,128)(2,1)} custom-call(bf16[16,3,640]{2,1,0:T(4,128)(2,1)} %reshape.140.source), custom_call_target="tpu_custom_call" | custom-call | tf_op jit(solution)/shard_map/pallas_call | solution.py:64
  30.4 0.8 fusion.60
  31.2 0.7 exp.32
  31.8 0.1 fusion.38
  32.0 1.8 %subtract_exponential_fusion = (f32[3,64]{1,0:T(4,128)}, f32[3,64]{1,0:T(4,128)S(1)}) fusion(f32[3,64]{1,0:T(4,128)} %param.36, f32[64]{0:T(128)S(1)} %exp.32, f32[64]{0:T(128)} %param.34, bf16[2048,64]{0,1:T(8,128)(2,1)} %param.33, bf16[3,2048]{1,0:T(4,128)(2,1)S(1)} %copy-done.8, f32[2048]{0:T(1024)} %param.40, f32[3]{0:T(128)S(1)} %add_rsqrt_fusion.3), kind=kOutput, calls=%fused_computation.89 | convolution fusion | flops 812736 | bytes 285452 | tf_op jit(solution)/shard_map/dot_general | solution.py:24
  33.8 0.9 slice_bitcast_fusion.1
  34.7 0.1 reshape.143
  34.8 0.1 reshape.142
  34.9 0.8 convert_element_type.112
  35.8 0.3 multiply_reduce_fusion.1
  36.2 0.1 reshape.144
  36.3 0.1 copy.43
  36.5 0.7 multiply_bitcast_fusion.inputs
  37.2 0.6 reshape_reshape.6.write
  37.9 0.6 reshape_reshape.7.read
  38.5 8.0 %shard_map.267 = (f32[3,64,64,128]{3,2,1,0:T(8,128)}, f32[3,2,64,32]{3,2,1,0:T(8,128)}) custom-call(f32[3,64]{1,0:T(4,128)} %get-tuple-element.15.decay, f32[3,2,64,32]{3,2,1,0:T(8,128)} %multiply_bitcast_fusion.inputs, f32[3,2,4,128]{3,2,1,0:T(4,128)} %reshape_reshape.6.write, f32[3,2,4,128]{3,2,1,0:T(4,128)} %reshape_reshape.7.read, f32[3,64,64,128]{3,2,1,0:T(8,128)} %carried.1), custom_call_target="tpu_custom_call" | custom-call | tf_op jit(solution)/shard_map/pallas_call | solution.py:131
  46.5 1.1 copy.44
  47.6 0.1 reshape.145
  47.9 0.1 bitcast_reduce_fusion
  48.1 0.6 multiply_convert_fusion.1.source
  48.8 15.1 %shard_map.268 = bf16[16,3,4096]{2,1,0:T(4,128)(2,1)} custom-call(bf16[3,4096]{1,0:T(4,128)(2,1)} %multiply_convert_fusion.1.source), custom_call_target="tpu_custom_call" | custom-call | tf_op jit(solution)/shard_map/pallas_call | solution.py:64
  63.9 1.4 %reshape.146 = bf16[48,4096]{1,0:T(8,128)(2,1)S(1)} reshape(bf16[16,3,4096]{2,1,0:T(4,128)(2,1)} %shard_map.268) | data formatting | bytes 786432 | tf_op jit(solution)/shard_map/reshape | solution.py:226
  65.3 1.5 %fusion.14.source = bf16[48,128]{1,0:T(8,128)(2,1)S(1)} fusion(bf16[48,4096]{1,0:T(8,128)(2,1)S(1)} %reshape.146, bf16[4096,128]{1,0:T(8,128)(2,1)} %param.42, f32[48,2048]{1,0:T(8,128)S(1)} %reshape.148, s32[]{:T(128)S(6)} %select_n.20), kind=kOutput, calls=%fused_computation.15 | convolution fusion | flops 50343936 | bytes 1478660 | tf_op jit(solution)/shard_map/dot_general | solution.py:24
  66.9 0.1 convolution_convert_fusion.1
  67.1 0.1 convolution_convert_fusion.2
  67.2 0.2 copy-done.5
  67.4 12.1 %shard_map.269 = bf16[16,48,128]{2,1,0:T(8,128)(2,1)} custom-call(bf16[48,128]{1,0:T(8,128)(2,1)} %copy-done.5), custom_call_target="tpu_custom_call" | custom-call | tf_op jit(solution)/shard_map/pallas_call | solution.py:64
  79.5 1.1 %fusion.20 = f32[48]{0:T(128)S(1)} fusion(bf16[16,48,128]{2,1,0:T(8,128)(2,1)} %shard_map.269), kind=kLoop, calls=%fused_computation.30 | loop fusion | flops 294864 | bytes 196800 | tf_op jit(solution)/shard_map/reduce_sum | solution.py:20
  80.7 2.2 %fusion.4 = f32[48,512]{1,0:T(8,128)S(1)} fusion(bf16[1,2048,512]{2,1,0:T(8,128)(2,1)} %param.46, bf16[16,48,128]{2,1,0:T(8,128)(2,1)} %shard_map.269, f32[16,128]{1,0:T(8,128)S(1)} %bitcast.81, f32[48]{0:T(128)S(1)} %add_rsqrt_fusion.2), kind=kOutput, calls=%fused_computation.6 | convolution fusion | flops 101056512 | bytes 2400448 | tf_op jit(solution)/shard_map/dot_general | solution.py:24
  82.9 2.5 %convolution_convert_fusion = bf16[48,2048]{1,0:T(8,128)(2,1)S(1)} fusion(bf16[1,512,2048]{2,1,0:T(8,128)(2,1)S(1)} %copy-done, bf16[1,2048,512]{2,1,0:T(8,128)(2,1)} %param.47, f32[48,512]{1,0:T(8,128)S(1)} %fusion.4, bf16[16,48,128]{2,1,0:T(8,128)(2,1)S(1)} %copy-done.1, f32[16,128]{1,0:T(8,128)S(1)} %bitcast.82, f32[48]{0:T(128)S(1)} %add_rsqrt_fusion.2), kind=kOutput, calls=%fused_computation | convolution fusion | flops 201965568 | bytes 4694208 | tf_op jit(solution)/shard_map/dot_general | solution.py:24
  85.5 0.9 reshape.147.source
  86.4 14.1 %shard_map.270 = bf16[16,3,3072]{2,1,0:T(4,128)(2,1)} custom-call(bf16[16,3,3072]{2,1,0:T(4,128)(2,1)} %reshape.147.source), custom_call_target="tpu_custom_call" | custom-call | tf_op jit(solution)/shard_map/pallas_call | solution.py:64
  100.6 1.1 convert_element_type.129
  101.7 0.8 copy_bitcast_fusion
  102.6 1.2 %fusion.61 = (f32[3]{0:T(128)S(1)}, f32[3,16]{1,0:T(4,128)S(1)}) fusion(pred[3,16]{1,0:T(4,128)(4,1)S(1)} %fusion.46, bf16[2048,16]{0,1:T(8,128)(2,1)S(1)} %copy-done.14, f32[48,2048]{1,0:T(8,128)} %copy_bitcast_fusion, s32[]{:T(128)S(6)} %select_n.22, f32[2048]{0:T(1024)S(1)} %copy-done.9, f32[3]{0:T(128)S(1)} %dynamic-slice.4), kind=kOutput, calls=%fused_computation.98 | convolution fusion | flops 215277 | bytes 106764 | tf_op jit(solution)/shard_map/dot_general | solution.py:24
  103.9 0.2 fusion.19
  104.2 2.6 %fusion = bf16[3,2048]{1,0:T(4,128)(2,1)} fusion(bf16[512,2048]{1,0:T(8,128)(2,1)} %param.51, f32[3,2048]{1,0:T(4,128)S(1)} %fusion.19, f32[48,2048]{1,0:T(8,128)} %copy_bitcast_fusion, s32[]{:T(128)S(6)} %select_n.22, f32[3,1024]{1,0:T(4,128)S(1)} %slice_reduce_fusion, f32[3]{0:T(128)S(1)} %dynamic-slice.4), kind=kOutput, calls=%fused_computation.2 | convolution fusion | flops 6322176 | bytes 2170896 | tf_op jit(solution)/shard_map/dot_general | solution.py:24
  106.8 0.9 fusion.30
  (54 shorter events, 1.3 us)
Async XLA Ops:
  0.6 82.3 %copy-start = (bf16[1,512,2048]{2,1,0:T(8,128)(2,1)S(1)}, bf16[1,512,2048]{2,1,0:T(8,128)(2,1)}, u32[]{:S(2)}) copy-start(bf16[1,512,2048]{2,1,0:T(8,128)(2,1)} %param.48) | copy-start | bytes 6291460
  0.6 18.4 %copy-start.2 = (bf16[2048,256]{1,0:T(8,128)(2,1)S(1)}, bf16[2048,256]{1,0:T(8,128)(2,1)}, u32[]{:S(2)}) copy-start(bf16[2048,256]{1,0:T(8,128)(2,1)} %param.30) | copy-start | bytes 3145732
  15.7 3.6 %copy-start.3 = (bf16[2048,256]{1,0:T(8,128)(2,1)S(1)}, bf16[2048,256]{1,0:T(8,128)(2,1)}, u32[]{:S(2)}) copy-start(bf16[2048,256]{1,0:T(8,128)(2,1)} %param.29) | copy-start | bytes 3145732
  16.6 15.2 %copy-start.8 = (bf16[3,2048]{1,0:T(4,128)(2,1)S(1)}, bf16[3,2048]{1,0:T(4,128)(2,1)}, u32[]{:S(2)}) copy-start(bf16[3,2048]{1,0:T(4,128)(2,1)} %source.1) | copy-start | bytes 36868
  19.3 16.4 %copy-start.4 = (bf16[3,3,6144]{2,1,0:T(4,128)(2,1)S(1)}, bf16[3,3,6144]{2,1,0:T(4,128)(2,1)}, u32[]{:S(2)}) copy-start(bf16[3,3,6144]{2,1,0:T(4,128)(2,1)} %param.27) | copy-start | bytes 331780
  19.3 16.8 %copy-start.10 = (f32[6144]{0:T(1024)S(1)}, f32[6144]{0:T(1024)}, u32[]{:S(2)}) copy-start(f32[6144]{0:T(1024)} %param.39) | copy-start | bytes 73732
  38.5 9.2 %copy-start.13 = (f32[64]{0:T(128)S(1)}, f32[64]{0:T(128)}, u32[]{:S(2)}) copy-start(f32[64]{0:T(128)} %param.37) | copy-start | bytes 772
  38.5 9.7 %copy-start.11 = (f32[4096]{0:T(1024)S(1)}, f32[4096]{0:T(1024)}, u32[]{:S(2)}) copy-start(f32[4096]{0:T(1024)} %param.41) | copy-start | bytes 49156
  46.5 20.3 %copy-start.9 = (f32[2048]{0:T(1024)S(1)}, f32[2048]{0:T(1024)}, u32[]{:S(2)}) copy-start(f32[2048]{0:T(1024)} %param.43) | copy-start | bytes 24580
  46.5 20.4 %copy-start.6 = (bf16[128,512]{1,0:T(8,128)(2,1)S(1)}, bf16[128,512]{1,0:T(8,128)(2,1)}, u32[]{:S(2)}) copy-start(bf16[128,512]{1,0:T(8,128)(2,1)} %param.50) | copy-start | bytes 393220
  47.6 19.5 %copy-start.7 = (bf16[128,512]{1,0:T(8,128)(2,1)S(1)}, bf16[128,512]{1,0:T(8,128)(2,1)}, u32[]{:S(2)}) copy-start(bf16[128,512]{1,0:T(8,128)(2,1)} %param.49) | copy-start | bytes 393220
  66.8 0.6 copy-start.5
  79.5 3.4 %copy-start.1 = (bf16[16,48,128]{2,1,0:T(8,128)(2,1)S(1)}, bf16[16,48,128]{2,1,0:T(8,128)(2,1)}, u32[]{:S(2)}) copy-start(bf16[16,48,128]{2,1,0:T(8,128)(2,1)} %shard_map.269) | copy-start | bytes 589828
  85.5 16.2 %copy-start.12 = (s32[3,6]{1,0:T(4,128)S(1)}, s32[3,6]{1,0:T(4,128)}, u32[]{:S(2)}) copy-start(s32[3,6]{1,0:T(4,128)} %param.45) | copy-start | bytes 220
  85.5 17.1 %copy-start.14 = (bf16[2048,16]{0,1:T(8,128)(2,1)S(1)}, bf16[2048,16]{0,1:T(8,128)(2,1)}, u32[]{:S(2)}) copy-start(bf16[2048,16]{0,1:T(8,128)(2,1)} %param.44) | copy-start | bytes 196612
where the time goes:
time: 109 us; the launch traced here: 108 us
  Pallas kernels  71.9 us (66%)
  matrix products  15.2 us (14%)
  other arithmetic  10.1 us (9%)
  local copies, waits for them, and re-layouts  9.48 us (9%)
    pallas_call x5, Pallas kernels, send(): pl.pallas_call(functools.partial(exchange_kernel, n, spread), out_shape=j...  63.9 us
    dot_general x12, matrix products, matmul(): return jnp.dot(left, right, preferred_element_type=jnp.float32)  15.2 us
    pallas_call x1, Pallas kernels, state_step(): pl.pallas_call(functools.partial(state_kernel, head_count // groups), gri...  8 us
    reduce_sum x4, other arithmetic, row_scale(): jnp.mean(values * values, axis=-1, keepdims=True) + epsilon  2.54 us

commit v1 on v0

--- a/solution.py
+++ b/solution.py
@@ -1,4 +1,5 @@
 import functools
+import typing
 
 import jax
 import jax.numpy as jnp
@@ -261,6 +262,578 @@
     return (layer_out, next_state, window[:, 1:])
 
 
+def dot_t(left, right):
+    return lax.dot_general(left, right, (((1,), (1,)), ((), ())), preferred_element_type=jnp.float32)
+
+
+def dot_0(left, right):
+    return lax.dot_general(left, right, (((0,), (0,)), ((), ())), preferred_element_type=jnp.float32)
+
+
+def silu(v):
+    return v / (1.0 + jnp.exp(-v))
+
+
+def split2(v):
+    high = v.astype(jnp.bfloat16)
+    return high, (v - high.astype(jnp.float32)).astype(jnp.bfloat16)
+
+
+class Args(typing.NamedTuple):
+    hidden: typing.Any
+    conv_window: typing.Any
+    ssm_state: typing.Any
+    gate_proj: typing.Any
+    input_proj: typing.Any
+    write_t: typing.Any
+    read_t: typing.Any
+    step_t: typing.Any
+    step_bias: typing.Any
+    decay_log: typing.Any
+    decay_shift: typing.Any
+    skip_scale: typing.Any
+    conv_taps: typing.Any
+    conv_bias: typing.Any
+    mix_gain: typing.Any
+    group_gain: typing.Any
+    out_proj: typing.Any
+    ffn_gain: typing.Any
+    router_t: typing.Any
+    expert_ids: typing.Any
+    expert_gate: typing.Any
+    expert_up: typing.Any
+    expert_down: typing.Any
+    shared_gate: typing.Any
+    shared_up: typing.Any
+    shared_down: typing.Any
+
+
+def layer_kernel(n, rows, *refs):
+    count = len(Args._fields)
+    hbm = Args(*refs[:count])
+    layer_out, next_state, next_window = refs[count : count + 3]
+    vm = Args(*refs[count + 3 : 2 * count + 3])
+    (
+        src1, land1, src2, land2, src3, land3, src4, land4, src5, land5, src6, land6,
+        fold1, fold3, fold5, x_all, x_low, p_all, extra, g_all, g_low, h_all, flag0, flag2, part48,
+        acc_gate, acc_up, base, cols, y_all, fresh, xv, wv, rv, step_x, skip_x,
+        decay_col, decayed, window, slots, served_f, in_sem, send_sem, recv_sem, pass_send, pass_recv,
+    ) = refs[2 * count + 3 :]
+    me = lax.axis_index("ep")
+    f32, bf16 = jnp.float32, jnp.bfloat16
+    width = vm.hidden.shape[1]
+    inner = cols.shape[1]
+    total = n * rows
+    heads = hbm.step_bias.shape[1]
+    head_dim = inner // heads
+    groups = GROUPS
+    per_group = heads // groups
+    span = inner // groups
+    state = STATE
+    gate_cols = hbm.gate_proj.shape[1]
+    vec_cols = hbm.write_t.shape[0]
+    col_width = hbm.out_proj.shape[1]
+    shared_units = hbm.shared_gate.shape[1]
+
+    def flipped(value):
+        other = me
+        bit = 1
+        while bit < n:
+            if value & bit:
+                other = other + bit - 2 * bit * lax.rem(me // bit, 2)
+            bit *= 2
+        return other
+
+    far_first = tuple(range(n - 1, 0, -1))
+    partner = flipped(1)
+
+    barrier = pltpu.get_barrier_semaphore()
+    for step in far_first:
+        pl.semaphore_signal(
+            barrier, inc=1, device_id={"ep": flipped(step)}, device_id_type=pl.DeviceIdType.MESH
+        )
+    loads = Args(
+        *[pltpu.make_async_copy(there, here, in_sem.at[at]) for at, (there, here) in enumerate(zip(hbm, vm))]
+    )
+    for one in (
+        loads.hidden,
+        loads.mix_gain,
+        loads.expert_ids,
+        loads.gate_proj,
+        loads.input_proj,
+        loads.write_t,
+        loads.read_t,
+        loads.step_t,
+        loads.step_bias,
+        loads.decay_log,
+        loads.decay_shift,
+        loads.skip_scale,
+        loads.conv_window,
+        loads.conv_taps,
+        loads.conv_bias,
+        loads.ssm_state,
+        loads.group_gain,
+        loads.out_proj,
+        loads.shared_gate,
+        loads.shared_up,
+        loads.ffn_gain,
+        loads.expert_gate,
+        loads.expert_up,
+        loads.expert_down,
+        loads.router_t,
+        loads.shared_down,
+    ):
+        one.start()
+
+    def need(*these):
+        for one in these:
+            one.wait()
+
+    def remote(source, target_ref, sends, arrives, target):
+        return pltpu.make_async_remote_copy(
+            src_ref=source,
+            dst_ref=target_ref,
+            send_sem=sends,
+            recv_sem=arrives,
+            device_id={"ep": target},
+            device_id_type=pl.DeviceIdType.MESH,
+        )
+
+    sent = []
+
+    def begin(one):
+        one.start()
+        sent.append(one)
+        return one
+
+    def spread(phase, source, landed):
+        steps = far_first[:: 2] if n % 2 else tuple(range(n - 2, 0, -2))
+        out = {}
+        for step in steps:
+            out[step] = begin(
+                remote(source, landed.at[me], send_sem.at[phase, step], recv_sem.at[phase, step], flipped(step))
+            )
+        out[0] = begin(remote(source, landed.at[me], pass_send.at[phase, 0], pass_recv.at[phase, 0], partner))
+        return out
+
+    def collect(phase, landed, out, take):
+        passed = [(partner, out[0])]
+        for step in range(2, n, 2):
+            out[step].wait_recv()
+            owner = flipped(step)
+            block = landed.at[owner]
+            passed.append(
+                (
+                    flipped(step + 1),
+                    begin(remote(block, block, pass_send.at[phase, step], pass_recv.at[phase, step], partner)),
+                )
+            )
+            take(owner)
+        for owner, one in passed:
+            one.wait_recv()
+            take(owner)
+
+    def scatter(phase, source, landed):
+        return {
+            step: begin(
+                remote(
+                    source.at[flipped(step)], landed.at[me], send_sem.at[phase, step], recv_sem.at[phase, me],
+                    flipped(step),
+                )
+            )
+            for step in far_first
+        }
+
+    def arrived(phase, source, landed, place):
+        @pl.when(me != place)
+        def _():
+            remote(
+                source, landed.at[place], send_sem.at[phase, 0], recv_sem.at[phase, place], place
+            ).wait_recv()
+
+    def folded(value, buffer):
+        wide = buffer.shape[1]
+        rest = wide // rows
+        buffer[0:rows] = value[:, :wide]
+        for row in range(rows):
+            buffer[rows : rows + 1, row * rest : (row + 1) * rest] = value[row : row + 1, wide:]
+        return buffer[...].astype(bf16)
+
+    def unfolded(landed, owner, target):
+        piece = landed[owner].astype(f32)
+        wide = piece.shape[1]
+        rest = wide // rows
+        target[owner, 0:rows, :wide] = piece[0:rows]
+        for row in range(rows):
+            target[owner, row : row + 1, wide:] = piece[rows : rows + 1, row * rest : (row + 1) * rest]
+
+    need(loads.hidden, loads.mix_gain, loads.expert_ids)
+    own = vm.hidden[...].astype(f32)
+    scale = lax.rsqrt(jnp.mean(own * own, axis=-1, keepdims=True) + epsilon)
+    normed = (own * scale * vm.mix_gain[...]).astype(bf16)
+    packed = folded(normed.astype(f32), fold1)
+    src1[...] = packed
+    land1[me] = packed
+    pl.semaphore_wait(barrier, n - 1)
+    rows1 = spread(0, src1, land1)
+
+    lane = lax.broadcasted_iota(jnp.int32, (rows, 128), 1)
+    ids = vm.expert_ids[...]
+    chosen = jnp.zeros((rows, 128), f32)
+    for k in range(ids.shape[1]):
+        chosen = jnp.where(lane == ids[:, k : k + 1], 1.0, chosen)
+    for place in range(n):
+        for row in range(rows):
+            extra[place, rows : rows + 1, row * col_width : (row + 1) * col_width] = own[
+                row : row + 1, place * col_width : (place + 1) * col_width
+            ]
+        extra[place, rows : rows + 1, rows * col_width : rows * col_width + 128] = chosen[0:1]
+        extra[place, rows : rows + 1, rows * col_width + 128 : rows * col_width + 256] = chosen[2:3]
+    need(loads.step_t, loads.step_bias, loads.decay_log, loads.decay_shift, loads.skip_scale)
+    raw = dot_t(normed, vm.step_t[...]) + vm.step_bias[...]
+    step_size = jnp.maximum(raw, 0.0) + jnp.log1p(jnp.exp(-jnp.abs(raw)))
+    decay = jnp.exp(vm.decay_shift[...] - step_size * jnp.exp(vm.decay_log[...]))
+    skip = vm.skip_scale[...]
+    low_half = lax.broadcasted_iota(jnp.int32, (rows, 128), 1) < head_dim
+    for pair in range(heads // 2):
+        at = slice(pair * 128, (pair + 1) * 128)
+        first = jnp.broadcast_to(step_size[:, 2 * pair : 2 * pair + 1], (rows, 128))
+        second = jnp.broadcast_to(step_size[:, 2 * pair + 1 : 2 * pair + 2], (rows, 128))
+        step_x[:, at] = jnp.where(low_half, first, second)
+        first = jnp.broadcast_to(skip[:, 2 * pair : 2 * pair + 1], (1, 128))
+        second = jnp.broadcast_to(skip[:, 2 * pair + 1 : 2 * pair + 2], (1, 128))
+        skip_x[:, at] = jnp.where(low_half[0:1], first, second)
+    for row in range(rows):
+        spread_row = jnp.broadcast_to(jnp.concatenate([decay[row : row + 1]] * 2, axis=1), (128, 128))
+        turned = spread_row.T
+        for group in range(groups):
+            decay_col[row * groups + group] = turned[group * per_group : (group + 1) * per_group]
+
+    need(loads.conv_window, loads.conv_taps, loads.conv_bias)
+    taps = vm.conv_taps[...].astype(f32)
+    for row in range(rows):
+        old = vm.conv_window[row].astype(f32)
+        base[row : row + 1] = (
+            jnp.sum(old * taps[:3], axis=0, keepdims=True) + vm.conv_bias[...]
+        )
+        window[row, 0:2] = old[1:3]
+
+    unfolded(land1, me, x_all)
+    collect(0, land1, rows1, lambda owner: unfolded(land1, owner, x_all))
+    need(loads.gate_proj, loads.input_proj, loads.write_t, loads.read_t)
+    x_low[...] = x_all[...].reshape(x_low.shape).astype(bf16)
+    p_all[:, :gate_cols] = matmul(x_low[...], vm.gate_proj[...])
+    p_all[:, gate_cols : 2 * gate_cols] = matmul(x_low[...], vm.input_proj[...])
+    p_all[:, 2 * gate_cols : 2 * gate_cols + vec_cols] = dot_t(x_low[...], vm.write_t[...])
+    p_all[:, 2 * gate_cols + vec_cols :] = dot_t(x_low[...], vm.read_t[...])
+    own_part = lax.broadcasted_iota(jnp.int32, extra.shape[1:], 0) < rows
+    for place in range(n):
+        src2[place] = jnp.where(own_part, p_all[8 * place : 8 * place + rows + 1], extra[place]).astype(bf16)
+    scatter(1, src2, land2)
+    land2[me] = src2[me]
+
+    need(loads.ssm_state)
+
+    def decay_group(at, carry):
+        columns = decay_col[at]
+        for head in range(per_group):
+            part = slice(head * head_dim, (head + 1) * head_dim)
+            value = vm.ssm_state[at, part] * columns[head : head + 1]
+            next_state[at, part] = value
+            decayed[at, part] = value.astype(bf16)
+        return carry
+
+    lax.fori_loop(0, rows * groups, decay_group, 0)
+
+    need(loads.group_gain)
+    half = vec_cols
+    for place in range(0, n, 2):
+        last = []
+        for one in (place, place + 1):
+            arrived(1, src2.at[0], land2, one)
+            whole = land2[one].astype(f32)
+            piece = whole[0:rows]
+            at = slice(one * gate_cols, (one + 1) * gate_cols)
+            cols[:, at] = piece[:, :gate_cols]
+            fresh[:, at] = piece[:, gate_cols : 2 * gate_cols]
+            last.append(piece[:, 2 * gate_cols :])
+            for row in range(rows):
+                h_all[8 * one + row : 8 * one + row + 1] = whole[
+                    rows : rows + 1, row * col_width : (row + 1) * col_width
+                ]
+            flag0[one : one + 1] = whole[rows : rows + 1, rows * col_width : rows * col_width + 128]
+            flag2[one : one + 1] = whole[rows : rows + 1, rows * col_width + 128 : rows * col_width + 256]
+        low = lax.broadcasted_iota(jnp.int32, last[0].shape, 1) < half
+        at = slice(inner + place * half, inner + (place + 2) * half)
+        fresh[:, at] = jnp.where(low, last[0], pltpu.roll(last[1], half, 1))
+        at = slice(at.start + groups * state, at.stop + groups * state)
+        fresh[:, at] = jnp.where(low, pltpu.roll(last[0], half, 1), last[1])
+    convolved = silu(base[...] + fresh[...] * taps[3:4])
+    head_input = convolved[:, :inner]
+    xv[...] = head_input
+    for group in range(groups):
+        at = slice(inner + group * state, inner + (group + 1) * state)
+        write = convolved[:, at]
+        read = convolved[:, at.start + groups * state : at.stop + groups * state]
+        wv[group] = write
+        rv[group] = read
+    for group in range(groups):
+        read = rv[group]
+        high, low = split2(read)
+        for row in range(rows):
+            left = jnp.concatenate([high[row : row + 1], low[row : row + 1]], axis=0)
+            both = dot_t(left, decayed[row * groups + group])
+            y_all[row : row + 1, group * span : (group + 1) * span] = both[0:1] + both[1:2]
+    for group in range(groups):
+        at = slice(group * span, (group + 1) * span)
+        overlap = jnp.sum(wv[group] * rv[group], axis=1, keepdims=True)
+        mixed = y_all[:, at] + xv[:, at] * (step_x[:, at] * overlap + skip_x[:, at])
+        mixed = mixed.astype(bf16).astype(f32) * silu(cols[:, at])
+        mixed = mixed * lax.rsqrt(jnp.mean(mixed * mixed, axis=-1, keepdims=True) + epsilon)
+        y_all[:, at] = mixed * vm.group_gain[:, at]
+    packed = folded(y_all[...], fold3)
+    src3[...] = packed
+    land3[me] = packed
+    rows3 = spread(2, src3, land3)
+
+    for group in range(groups):
+        at = slice(group * span, (group + 1) * span)
+        high, low = split2(xv[:, at] * step_x[:, at])
+        left = jnp.concatenate([high.astype(f32), low.astype(f32), high.astype(f32)], axis=0).astype(bf16)
+        w_high, w_low = split2(wv[group])
+        right = jnp.concatenate([w_high.astype(f32), w_high.astype(f32), w_low.astype(f32)], axis=0)
+        owner = lax.rem(lax.broadcasted_iota(jnp.int32, right.shape, 0), rows)
+        for row in range(rows):
+            picked = jnp.where(owner == row, right, 0.0).astype(bf16)
+            place = row * groups + group
+            next_state[place] = next_state[place] + dot_0(left, picked)
+    for row in range(rows):
+        window[row, 2:3] = fresh[row : row + 1]
+        next_window[row] = window[row].astype(bf16)
+
+    slot_row = lax.broadcasted_iota(jnp.int32, (2 * n, total), 0)
+    slot_lane = lax.broadcasted_iota(jnp.int32, (2 * n, total), 1)
+    first_row = (slot_row // 2) * rows
+    even = slot_row % 2 == 0
+    outer = jnp.where(even, first_row, first_row + 2)
+    whose = lax.broadcasted_iota(jnp.int32, (2 * n, n), 1) == lax.broadcasted_iota(jnp.int32, (2 * n, n), 0) // 2
+    whose = jnp.where(whose, 1.0, 0.0).astype(bf16)
+    even_row = lax.broadcasted_iota(jnp.int32, (2 * n, 128), 0) % 2 == 0
+    flag = jnp.where(
+        even_row, matmul(whose, flag0[...].astype(bf16)), matmul(whose, flag2[...].astype(bf16))
+    )
+    flag = jnp.where(lax.broadcasted_iota(jnp.int32, flag.shape, 1) == me, flag, 0.0)
+    flag = jnp.sum(flag, axis=1, keepdims=True)
+    source_row = jnp.where(flag > 0.5, outer, first_row + 1)
+    select = jnp.where(slot_lane == source_row, 1.0, 0.0).astype(bf16)
+
+    unfolded(land3, me, g_all)
+    collect(2, land3, rows3, lambda owner: unfolded(land3, owner, g_all))
+    need(loads.out_proj, loads.shared_gate, loads.shared_up, loads.ffn_gain)
+    g_low[...] = g_all[...].reshape(g_low.shape).astype(bf16)
+    resid_f = h_all[...] + matmul(g_low[...], vm.out_proj[...])
+    for place in range(n):
+        part48[place * rows : (place + 1) * rows] = resid_f[8 * place : 8 * place + rows]
+    resid_part = part48[...].astype(bf16)
+    src4[...] = resid_part
+    land4[me] = resid_part
+    rows4 = spread(3, src4, land4)
+    gain_part = vm.ffn_gain[:, pl.ds(pl.multiple_of(me * col_width, col_width), col_width)]
+    shared_part = (resid_part.astype(f32) * gain_part).astype(bf16)
+    slots[:, :shared_units] = matmul(shared_part, vm.shared_gate[...])
+    slots[:, shared_units:] = matmul(shared_part, vm.shared_up[...])
+    for place in range(n):
+        src5[place] = folded(slots[place * rows : (place + 1) * rows], fold5.at[place])
+    scatter(4, src5, land5)
+    land5[me] = src5[me]
+
+    need(loads.expert_gate, loads.expert_up, loads.expert_down)
+    acc_gate[...] = jnp.zeros_like(acc_gate)
+    acc_up[...] = jnp.zeros_like(acc_up)
+    squares = [jnp.zeros((total, col_width), f32)]
+
+    def add_block(owner):
+        piece = land4[owner].astype(f32)
+        squares[0] = squares[0] + piece * piece
+        at = pl.ds(pl.multiple_of(owner * col_width, col_width), col_width)
+        scaled = (piece * vm.ffn_gain[:, at]).astype(bf16)
+        acc_gate[...] += matmul(scaled, vm.expert_gate[at])
+        acc_up[...] += matmul(scaled, vm.expert_up[at])
+
+    add_block(me)
+    collect(3, land4, rows4, add_block)
+    scale_all = lax.rsqrt(jnp.sum(squares[0], axis=1, keepdims=True) / width + epsilon)
+    hidden_units = (silu(acc_gate[...] * scale_all) * (acc_up[...] * scale_all)).astype(bf16)
+    served = matmul(select, hidden_units).astype(bf16)
+    served_f[...] = matmul(served, vm.expert_down[...])
+    for place in range(n):
+        src6[place] = served_f[2 * place : 2 * place + 2].astype(bf16)
+    scatter(5, src6, land6)
+    land6[me] = src6[me]
+
+    need(loads.router_t, loads.shared_down)
+    own_row = lax.broadcasted_iota(jnp.int32, (rows, total), 0) + me * rows
+    pick = jnp.where(lax.broadcasted_iota(jnp.int32, (rows, total), 1) == own_row, 1.0, 0.0).astype(bf16)
+    for place in range(n):
+        at = slice(place * col_width, (place + 1) * col_width)
+        y_all[:, at] = matmul(pick, land4[place])
+    resid_own = y_all[:, :width]
+    norm_scale = lax.rsqrt(jnp.mean(resid_own * resid_own, axis=-1, keepdims=True) + epsilon)
+    routed_own = (resid_own * norm_scale * vm.ffn_gain[...]).astype(bf16)
+    scores = 1.0 / (1.0 + jnp.exp(-dot_t(routed_own, vm.router_t[...])))
+    kept = chosen[:, :n]
+    scores = jnp.where(kept > 0.5, scores, 0.0)
+    weights = routed_scale * scores / jnp.sum(scores, axis=1, keepdims=True)
+    outer_w = jnp.concatenate([weights[0:1], weights[2:3]], axis=0)
+    middle = weights[1:2]
+    inner_w = jnp.concatenate([middle * (1.0 - kept[0:1]), middle * kept[0:1]], axis=0)
+    shared = jnp.zeros(fold5.shape[1:], f32)
+    for place in range(n):
+        arrived(4, src5.at[0], land5, place)
+        shared = shared + land5[place].astype(f32)
+    wide = shared.shape[1]
+    rest = wide // rows
+    cols[:, :wide] = shared[0:rows]
+    for row in range(rows):
+        cols[row : row + 1, wide : wide + rest] = shared[rows : rows + 1, row * rest : (row + 1) * rest]
+    shared = cols[:, : wide + rest] * norm_scale
+    shared_hidden = (silu(shared[:, :shared_units]) * shared[:, shared_units:]).astype(bf16)
+    start = resid_own + matmul(shared_hidden, vm.shared_down[...])
+    y_all[:, :width] = start
+    ends = jnp.zeros((2, width), f32)
+    mid = jnp.zeros((2, width), f32)
+    for place in range(n):
+        arrived(5, src6.at[0], land6, place)
+        piece = land6[place].astype(f32)
+        ends = ends + piece * outer_w[:, place : place + 1]
+        mid = mid + piece * inner_w[:, place : place + 1]
+    xv[0:1, :width] = ends[0:1]
+    xv[1:2, :width] = mid[0:1] + mid[1:2]
+    xv[2:3, :width] = ends[1:2]
+    layer_out[...] = (y_all[:, :width] + xv[:, :width]).astype(bf16)
+    for one in sent:
+        one.wait_send()
+
+
+def store_kernel(layer_out, next_state, next_window, layer_hbm, state_hbm, window_hbm, sems):
+    pieces = [(layer_out, layer_hbm), (next_window, window_hbm)]
+    pieces += [(next_state.at[at], state_hbm.at[at]) for at in range(next_state.shape[0])]
+    copies = [pltpu.make_async_copy(a, b, sems.at[at]) for at, (a, b) in enumerate(pieces)]
+    for one in copies:
+        one.start()
+    for one in copies:
+        one.wait()
+
+
+def one_kernel(*args):
+    named = Args(*args)
+    n = lax.axis_size("ep")
+    rows, width = named.hidden.shape
+    inner = named.gate_proj.shape[1] * n
+    total = n * rows
+    heads = named.step_bias.shape[0]
+    flat = lambda one: one.reshape(1, -1)
+    named = named._replace(
+        write_t=named.write_t.T,
+        read_t=named.read_t.T,
+        step_t=named.step_t.T,
+        router_t=named.router_t.T,
+        step_bias=flat(named.step_bias),
+        decay_log=flat(named.decay_log),
+        skip_scale=flat(named.skip_scale),
+        conv_bias=flat(named.conv_bias),
+        mix_gain=flat(named.mix_gain),
+        group_gain=flat(named.group_gain),
+        ffn_gain=flat(named.ffn_gain),
+        expert_gate=named.expert_gate[0],
+        expert_up=named.expert_up[0],
+        expert_down=named.expert_down[0],
+    )
+    state_shape = named.ssm_state.shape
+    span = inner // GROUPS
+    named = named._replace(ssm_state=named.ssm_state.reshape(rows * GROUPS, span, STATE))
+    conv_dim = named.conv_bias.shape[1]
+    cols = 2 * named.gate_proj.shape[1] + 2 * named.write_t.shape[0]
+    col_width = named.out_proj.shape[1]
+    shared_units = named.shared_gate.shape[1]
+    bf16, f32 = jnp.bfloat16, jnp.float32
+    V = pltpu.VMEM
+    scratch = [V(one.shape, one.dtype) for one in named]
+    units = 2 * shared_units
+    scratch += [
+        V((4, width * 3 // 4), bf16), V((n, 4, width * 3 // 4), bf16),
+        V((n, 4, cols), bf16), V((n, 4, cols), bf16),
+        V((4, inner * 3 // 4), bf16), V((n, 4, inner * 3 // 4), bf16),
+        V((total, col_width), bf16), V((n, total, col_width), bf16),
+        V((n, 4, units * 3 // 4), bf16), V((n, 4, units * 3 // 4), bf16),
+        V((n, 2, width), bf16), V((n, 2, width), bf16),
+        V((4, width * 3 // 4), f32), V((4, inner * 3 // 4), f32), V((n, 4, units * 3 // 4), f32),
+        V((n, 8, width), f32), V((n * 8, width), bf16), V((n * 8, cols), f32), V((n, 4, cols), f32),
+        V((n, 8, inner), f32), V((n * 8, inner), bf16), V((n * 8, col_width), f32),
+        V((n, 128), f32), V((n, 128), f32), V((total, col_width), f32),
+        V((total, shared_units), f32), V((total, shared_units), f32),
+        V((rows, conv_dim), f32), V((rows, inner), f32), V((rows, inner), f32), V((rows, conv_dim), f32),
+        V((rows, inner), f32), V((GROUPS, rows, STATE), f32), V((GROUPS, rows, STATE), f32),
+        V((rows, inner), f32), V((1, inner), f32),
+        V((rows * GROUPS, heads // GROUPS, 128), f32), V((rows * GROUPS, span, STATE), bf16),
+        V((rows, 3, conv_dim), f32), V((total, units), f32), V((2 * n, width), f32),
+        pltpu.SemaphoreType.DMA((len(named),)),
+        pltpu.SemaphoreType.DMA((6, n)),
+        pltpu.SemaphoreType.DMA((6, n)),
+        pltpu.SemaphoreType.DMA((6, n)),
+        pltpu.SemaphoreType.DMA((6, n)),
+    ]
+    layer_out, next_state, next_window = pl.pallas_call(
+        functools.partial(layer_kernel, n, rows),
+        out_shape=(
+            pltpu.VMEM((rows, width), bf16),
+            pltpu.VMEM(named.ssm_state.shape, f32),
+            pltpu.VMEM(named.conv_window.shape, bf16),
+        ),
+        in_specs=[pl.BlockSpec(memory_space=pltpu.HBM)] * len(named),
+        out_specs=tuple(pl.BlockSpec(memory_space=pltpu.VMEM) for _ in range(3)),
+        scratch_shapes=scratch,
+        compiler_params=pltpu.CompilerParams(
+            collective_id=0, has_side_effects=True, vmem_limit_bytes=36 * 1024 * 1024
+        ),
+    )(*[pltpu.with_memory_space_constraint(one, pltpu.HBM) for one in named])
+    outs = (layer_out, next_state, next_window)
+    layer_out, next_state, next_window = pl.pallas_call(
+        store_kernel,
+        out_shape=tuple(jax.ShapeDtypeStruct(one.shape, one.dtype) for one in outs),
+        in_specs=[pl.BlockSpec(memory_space=pltpu.VMEM)] * 3,
+        out_specs=tuple(pl.BlockSpec(memory_space=pltpu.HBM) for _ in range(3)),
+        scratch_shapes=[pltpu.SemaphoreType.DMA((2 + named.ssm_state.shape[0],))],
+        compiler_params=pltpu.CompilerParams(vmem_limit_bytes=1024 * 1024),
+    )(*outs)
+    return layer_out, next_state.reshape(state_shape), next_window
+
+
+def fits(args):
+    named = Args(*args)
+    n = lax.axis_size("ep")
+    return (
+        named.hidden.shape[0] == 3
+        and n & (n - 1) == 0
+        and 2 <= n <= 128
+        and named.hidden.shape[1] % 512 == 0
+        and 2 * named.gate_proj.shape[1] + 128 == 3 * 128 + 256
+        and named.expert_gate.shape[2] == named.shared_gate.shape[1]
+        and named.shared_gate.shape[1] % 256 == 0
+        and named.hidden.shape[1] <= named.group_gain.shape[0]
+        and named.out_proj.shape[1] == 128
+        and named.gate_proj.shape[1] % 128 == 0
+        and named.write_t.shape[1] == 64
+        and named.expert_gate.shape[0] == 1
+        and named.router_t.shape[1] == n
+        and HEAD_DIM * 2 == 128
+    )
+
+
+def body(*args):
+    return one_kernel(*args) if fits(args) else shards(*args)
+
+
 def solution(mesh):
     placed = (
         P(("grp", "ep"), None),
@@ -291,7 +864,7 @@
         P(),
     )
     return jax.shard_map(
-        shards,
+        body,
         mesh=mesh,
         in_specs=placed,
         out_specs=(

time: 109 us -> 44.1 us (0.40)
  Pallas kernels: 71.9 us -> 43.2 us
  matrix products: 15.2 us -> 0 us
  other arithmetic: 10.1 us -> 0 us
  local copies, waits for them, and re-layouts: 9.48 us -> 0 us
    pallas_call x6 -> x2, Pallas kernels: 71.9 us -> 43.2 us  [the longest x1 40.3 us: one_kernel(): pl.pallas_call(functools.partial(layer_kernel, n, rows), out_shape=(pltpu...]
    dot_general x12 -> x0, matrix products: 15.2 us -> none  [matmul(): return jnp.dot(left, right, preferred_element_type=jnp.float32)]
    convert_element_type x5 -> x0, other arithmetic: 4.17 us -> none  [the longest x1 1.07 us: shards(): back = exchange(jnp.concatenate([result, shared_pre], axis=1).reshape(-1,...]
    reshape x8 -> x0, local copies, waits for them, and re-layouts: 3.48 us -> none  [the longest x1 1.37 us: shards(): gather(gated_out, 2).reshape(-1, inner_width)]
    reduce_sum x7 -> x0, other arithmetic: 3.11 us -> none  [the longest x4 2.54 us: row_scale(): jnp.mean(values * values, axis=-1, keepdims=True) + epsilon]
    transpose x4 -> x0, local copies, waits for them, and re-layouts: 1.94 us -> none  [the longest x1 1.06 us: state_step(): mixed.transpose(0, 1, 3, 2).reshape(rows, head_count, head_dim)]
    another operation x2 -> x0, local copies, waits for them, and re-layouts: 1.24 us -> none  [the longest x1 0.62 us: state_step(): write_vec.reshape(vec_shape)]
    convert_element_type x1 -> x0, local copies, waits for them, and re-layouts: 1.1 us -> none  [shards(): gathered_wide = gathered.astype(jnp.float32)]
where the time goes in v1:
time: 44.1 us; the launch traced here: 43.8 us
  Pallas kernels  43.2 us (98%)
  between operations  0.65 us (1%)
    pallas_call x1, Pallas kernels, one_kernel(): pl.pallas_call(functools.partial(layer_kernel, n, rows), out_shape=(pltpu...  40.3 us
    pallas_call x1, Pallas kernels, one_kernel(): pl.pallas_call(store_kernel, out_shape=tuple((jax.ShapeDtypeStruct(one.sh...  2.91 us

profile of v1, /device:TPU:0, one launch (start us, length us, event | category | flops | bytes accessed | tf_op | source)
XLA Modules:
  0.0 43.8 jit_solution(1416423062157421601)
XLA Ops:
  0.6 40.3 %shard_map.265 = (bf16[3,2048]{1,0:T(4,128)(2,1)S(1)}, f32[24,512,128]{2,1,0:T(8,128)S(1)}, bf16[3,3,6144]{2,1,0:T(4,128)(2,1)S(1)}) custom-call(bf16[3,2048]{1,0:T(4,128)(2,1)} %refs_0_.1, bf16[3,3,6144]{2,1,0:T(4,128)(2,1)} %refs_1_.1, f32[24,512,128]{2,1,0:T(8,128)} %bitcast.16, bf16[2048,256]{1,0:T(8,128)(2,1)} %refs_3_.1, bf16[2048,256]{1,0:T(8,128)(2,1)} %refs_4_.1, ...), custom_call_target="tpu_custom_call" | custom-call | tf_op jit(solution)/shard_map/pallas_call | solution.py:786
  40.9 2.9 %shard_map.266 = (bf16[3,2048]{1,0:T(4,128)(2,1)}, f32[24,512,128]{2,1,0:T(8,128)}, bf16[3,3,6144]{2,1,0:T(4,128)(2,1)}) custom-call(bf16[3,2048]{1,0:T(4,128)(2,1)S(1)} %get-tuple-element.9.layer_out, f32[24,512,128]{2,1,0:T(8,128)S(1)} %get-tuple-element.10.next_state, bf16[3,3,6144]{2,1,0:T(4,128)(2,1)S(1)} %get-tuple-element.11.next_window), custom_call_target="tpu_custom_call" | custom-call | tf_op jit(solution)/shard_map/pallas_call | solution.py:801

commit v2 on v1

--- a/solution.py
+++ b/solution.py
@@ -314,10 +314,11 @@
     layer_out, next_state, next_window = refs[count : count + 3]
     vm = Args(*refs[count + 3 : 2 * count + 3])
     (
-        src1, land1, src2, land2, src3, land3, src4, land4, src5, land5, src6, land6,
-        fold1, fold3, fold5, x_all, x_low, p_all, extra, g_all, g_low, h_all, flag0, flag2, part48,
+        src1, land1, src2, land2, src_g, land_g, src3, land3, src4, land4, src5, land5, src6, land6,
+        fold1, fold3, fold5, x_all, x_low, p_all, gate_all, extra, g_all, g_low, h_all, flag0, flag2, part48,
         acc_gate, acc_up, base, cols, y_all, fresh, xv, wv, rv, step_x, skip_x,
-        decay_col, decayed, window, slots, served_f, in_sem, send_sem, recv_sem, pass_send, pass_recv,
+        decay_col, decayed, window, slots, served_f, vec_proj,
+        in_sem, send_sem, ring_sem, part_sem, whole_sem,
     ) = refs[2 * count + 3 :]
     me = lax.axis_index("ep")
     f32, bf16 = jnp.float32, jnp.bfloat16
@@ -399,57 +400,55 @@
             device_id_type=pl.DeviceIdType.MESH,
         )
 
-    sent = []
-
-    def begin(one):
-        one.start()
-        sent.append(one)
-        return one
-
-    def spread(phase, source, landed):
-        steps = far_first[:: 2] if n % 2 else tuple(range(n - 2, 0, -2))
+    blocks = []
+
+    def sends(phase, landed):
+        blocks.append((phase, landed))
+        return send_sem.at[phase]
+
+    def all_blocks(landed, sem, arrives):
+        many = landed.at[pl.ds(0, n - 1)]
+        return remote(many, many, sem, arrives, partner)
+
+    def spread(phase, ring, source, landed):
+        sem = sends(phase, landed)
         out = {}
-        for step in steps:
-            out[step] = begin(
-                remote(source, landed.at[me], send_sem.at[phase, step], recv_sem.at[phase, step], flipped(step))
-            )
-        out[0] = begin(remote(source, landed.at[me], pass_send.at[phase, 0], pass_recv.at[phase, 0], partner))
+        for step in range(n - 2, -1, -2):
+            out[step] = remote(source, landed.at[me], sem, ring_sem.at[ring, step + 1], flipped(step + 1))
+            out[step].start()
         return out
 
-    def collect(phase, landed, out, take):
+    def collect(phase, ring, landed, out, take):
         passed = [(partner, out[0])]
         for step in range(2, n, 2):
             out[step].wait_recv()
-            owner = flipped(step)
+            owner = flipped(step + 1)
             block = landed.at[owner]
-            passed.append(
-                (
-                    flipped(step + 1),
-                    begin(remote(block, block, pass_send.at[phase, step], pass_recv.at[phase, step], partner)),
-                )
-            )
-            take(owner)
+            one = remote(block, block, send_sem.at[phase], ring_sem.at[ring, step], partner)
+            one.start()
+            passed.append((flipped(step), one))
+            take(owner, 0)
+        return passed
+
+    def finish(passed, take):
         for owner, one in passed:
             one.wait_recv()
-            take(owner)
-
-    def scatter(phase, source, landed):
-        return {
-            step: begin(
-                remote(
-                    source.at[flipped(step)], landed.at[me], send_sem.at[phase, step], recv_sem.at[phase, me],
-                    flipped(step),
-                )
-            )
-            for step in far_first
-        }
-
-    def arrived(phase, source, landed, place):
+            take(owner, 0 if owner is partner else 1)
+
+    def scatter(phase, source, landed, sem):
+        sent = sends(phase, landed)
+        for step in far_first:
+            to = flipped(step)
+            remote(source.at[to], landed.at[me], sent, sem, to).start()
+
+    def arrived(part, landed, place):
         @pl.when(me != place)
         def _():
-            remote(
-                source, landed.at[place], send_sem.at[phase, 0], recv_sem.at[phase, place], place
-            ).wait_recv()
+            block = landed.at[place]
+            remote(block, block, send_sem.at[0], part_sem.at[part, place], place).wait_recv()
+
+    def arrived_all(which, landed):
+        all_blocks(landed, send_sem.at[0], whole_sem.at[which]).wait_recv()
 
     def folded(value, buffer):
         wide = buffer.shape[1]
@@ -459,13 +458,21 @@
             buffer[rows : rows + 1, row * rest : (row + 1) * rest] = value[row : row + 1, wide:]
         return buffer[...].astype(bf16)
 
-    def unfolded(landed, owner, target):
+    def unfolded(landed, owner, kind, target):
         piece = landed[owner].astype(f32)
         wide = piece.shape[1]
         rest = wide // rows
-        target[owner, 0:rows, :wide] = piece[0:rows]
+        chip = owner // 2
+        target[chip, 4 * kind : 4 * kind + rows, :wide] = piece[0:rows]
         for row in range(rows):
-            target[owner, row : row + 1, wide:] = piece[rows : rows + 1, row * rest : (row + 1) * rest]
+            target[chip, 4 * kind + row : 4 * kind + row + 1, wide:] = piece[
+                rows : rows + 1, row * rest : (row + 1) * rest
+            ]
+
+    def in_order(value):
+        tiles = value.reshape(n // 2, 8, value.shape[1])
+        turned = jnp.concatenate([tiles[:, 4:], tiles[:, :4]], axis=1)
+        return jnp.where(lax.rem(me, 2) == 1, tiles, turned).reshape(value.shape)
 
     need(loads.hidden, loads.mix_gain, loads.expert_ids)
     own = vm.hidden[...].astype(f32)
@@ -475,7 +482,7 @@
     src1[...] = packed
     land1[me] = packed
     pl.semaphore_wait(barrier, n - 1)
-    rows1 = spread(0, src1, land1)
+    rows1 = spread(0, 0, src1, land1)
 
     lane = lax.broadcasted_iota(jnp.int32, (rows, 128), 1)
     ids = vm.expert_ids[...]
@@ -487,8 +494,6 @@
             extra[place, rows : rows + 1, row * col_width : (row + 1) * col_width] = own[
                 row : row + 1, place * col_width : (place + 1) * col_width
             ]
-        extra[place, rows : rows + 1, rows * col_width : rows * col_width + 128] = chosen[0:1]
-        extra[place, rows : rows + 1, rows * col_width + 128 : rows * col_width + 256] = chosen[2:3]
     need(loads.step_t, loads.step_bias, loads.decay_log, loads.decay_shift, loads.skip_scale)
     raw = dot_t(normed, vm.step_t[...]) + vm.step_bias[...]
     step_size = jnp.maximum(raw, 0.0) + jnp.log1p(jnp.exp(-jnp.abs(raw)))
@@ -518,19 +523,28 @@
         )
         window[row, 0:2] = old[1:3]
 
-    unfolded(land1, me, x_all)
-    collect(0, land1, rows1, lambda owner: unfolded(land1, owner, x_all))
-    need(loads.gate_proj, loads.input_proj, loads.write_t, loads.read_t)
+    need(loads.write_t, loads.read_t)
+    vec_proj[...] = jnp.concatenate([vm.write_t[...], vm.read_t[...]], axis=0).T
+    unfolded(land1, me, 1, x_all)
+    take1 = lambda owner, kind: unfolded(land1, owner, kind, x_all)
+    finish(collect(0, 0, land1, rows1, take1), take1)
+    need(loads.gate_proj, loads.input_proj)
     x_low[...] = x_all[...].reshape(x_low.shape).astype(bf16)
-    p_all[:, :gate_cols] = matmul(x_low[...], vm.gate_proj[...])
-    p_all[:, gate_cols : 2 * gate_cols] = matmul(x_low[...], vm.input_proj[...])
-    p_all[:, 2 * gate_cols : 2 * gate_cols + vec_cols] = dot_t(x_low[...], vm.write_t[...])
-    p_all[:, 2 * gate_cols + vec_cols :] = dot_t(x_low[...], vm.read_t[...])
+    p_all[:, :gate_cols] = in_order(matmul(x_low[...], vm.input_proj[...]))
+    p_all[:, gate_cols:] = in_order(matmul(x_low[...], vec_proj[...]))
     own_part = lax.broadcasted_iota(jnp.int32, extra.shape[1:], 0) < rows
     for place in range(n):
-        src2[place] = jnp.where(own_part, p_all[8 * place : 8 * place + rows + 1], extra[place]).astype(bf16)
-    scatter(1, src2, land2)
+        src2[place] = jnp.where(own_part, p_all[4 * place : 4 * place + 4], extra[place]).astype(bf16)
+    scatter(1, src2, land2, part_sem.at[0, me])
     land2[me] = src2[me]
+    gate_all[...] = in_order(matmul(x_low[...], vm.gate_proj[...]))
+    ends = jnp.concatenate([chosen[0:1], chosen[2:3]], axis=1)
+    ends = jnp.broadcast_to(ends, (rows + 1, ends.shape[1]))
+    own_part = lax.broadcasted_iota(jnp.int32, ends.shape, 0) < rows
+    for place in range(n):
+        src_g[place] = jnp.where(own_part, gate_all[4 * place : 4 * place + 4], ends).astype(bf16)
+    scatter(2, src_g, land_g, whole_sem.at[0])
+    land_g[me] = src_g[me]
 
     need(loads.ssm_state)
 
@@ -540,29 +554,24 @@
             part = slice(head * head_dim, (head + 1) * head_dim)
             value = vm.ssm_state[at, part] * columns[head : head + 1]
             next_state[at, part] = value
-            decayed[at, part] = value.astype(bf16)
+        decayed[at] = next_state[at].T.astype(bf16)
         return carry
 
     lax.fori_loop(0, rows * groups, decay_group, 0)
 
-    need(loads.group_gain)
     half = vec_cols
     for place in range(0, n, 2):
         last = []
         for one in (place, place + 1):
-            arrived(1, src2.at[0], land2, one)
+            arrived(0, land2, one)
             whole = land2[one].astype(f32)
             piece = whole[0:rows]
-            at = slice(one * gate_cols, (one + 1) * gate_cols)
-            cols[:, at] = piece[:, :gate_cols]
-            fresh[:, at] = piece[:, gate_cols : 2 * gate_cols]
-            last.append(piece[:, 2 * gate_cols :])
+            fresh[:, one * gate_cols : (one + 1) * gate_cols] = piece[:, :gate_cols]
+            last.append(piece[:, gate_cols:])
             for row in range(rows):
-                h_all[8 * one + row : 8 * one + row + 1] = whole[
+                h_all[4 * one + row : 4 * one + row + 1] = whole[
                     rows : rows + 1, row * col_width : (row + 1) * col_width
                 ]
-            flag0[one : one + 1] = whole[rows : rows + 1, rows * col_width : rows * col_width + 128]
-            flag2[one : one + 1] = whole[rows : rows + 1, rows * col_width + 128 : rows * col_width + 256]
         low = lax.broadcasted_iota(jnp.int32, last[0].shape, 1) < half
         at = slice(inner + place * half, inner + (place + 2) * half)
         fresh[:, at] = jnp.where(low, last[0], pltpu.roll(last[1], half, 1))
@@ -577,24 +586,44 @@
         read = convolved[:, at.start + groups * state : at.stop + groups * state]
         wv[group] = write
         rv[group] = read
-    for group in range(groups):
-        read = rv[group]
-        high, low = split2(read)
+    def mix(group):
+        high, low = split2(rv[group])
         for row in range(rows):
             left = jnp.concatenate([high[row : row + 1], low[row : row + 1]], axis=0)
-            both = dot_t(left, decayed[row * groups + group])
+            both = matmul(left, decayed[row * groups + group])
             y_all[row : row + 1, group * span : (group + 1) * span] = both[0:1] + both[1:2]
-    for group in range(groups):
+
+    def gated(group):
         at = slice(group * span, (group + 1) * span)
         overlap = jnp.sum(wv[group] * rv[group], axis=1, keepdims=True)
         mixed = y_all[:, at] + xv[:, at] * (step_x[:, at] * overlap + skip_x[:, at])
         mixed = mixed.astype(bf16).astype(f32) * silu(cols[:, at])
         mixed = mixed * lax.rsqrt(jnp.mean(mixed * mixed, axis=-1, keepdims=True) + epsilon)
         y_all[:, at] = mixed * vm.group_gain[:, at]
-    packed = folded(y_all[...], fold3)
-    src3[...] = packed
-    land3[me] = packed
-    rows3 = spread(2, src3, land3)
+
+    def share(part):
+        packed = folded(y_all[:, part * half_inner : (part + 1) * half_inner], fold3)
+        src3[part] = packed
+        land3[part, me] = packed
+        return spread(3 + part, 1 + part, src3.at[part], land3.at[part])
+
+    half_inner = inner // 2
+    for group in range(groups // 2):
+        mix(group)
+    need(loads.group_gain)
+    arrived_all(0, land_g)
+    for place in range(n):
+        whole = land_g[place].astype(f32)
+        cols[:, place * gate_cols : (place + 1) * gate_cols] = whole[0:rows]
+        flag0[place : place + 1] = whole[rows : rows + 1, :128]
+        flag2[place : place + 1] = whole[rows : rows + 1, 128:]
+    for group in range(groups // 2):
+        gated(group)
+    rows3 = [share(0)]
+    for group in range(groups // 2, groups):
+        mix(group)
+        gated(group)
+    rows3.append(share(1))
 
     for group in range(groups):
         at = slice(group * span, (group + 1) * span)
@@ -627,24 +656,32 @@
     source_row = jnp.where(flag > 0.5, outer, first_row + 1)
     select = jnp.where(slot_lane == source_row, 1.0, 0.0).astype(bf16)
 
-    unfolded(land3, me, g_all)
-    collect(2, land3, rows3, lambda owner: unfolded(land3, owner, g_all))
-    need(loads.out_proj, loads.shared_gate, loads.shared_up, loads.ffn_gain)
-    g_low[...] = g_all[...].reshape(g_low.shape).astype(bf16)
-    resid_f = h_all[...] + matmul(g_low[...], vm.out_proj[...])
+    take3 = [lambda owner, kind, part=part: unfolded(land3.at[part], owner, kind, g_all.at[part]) for part in range(2)]
+    passed3 = []
+    for part in range(2):
+        take3[part](me, 1)
+        passed3.append(collect(3 + part, 1 + part, land3.at[part], rows3[part], take3[part]))
+    need(loads.out_proj)
+    resid_f = jnp.zeros(h_all.shape, f32)
+    for part in range(2):
+        finish(passed3[part], take3[part])
+        g_low[...] = g_all[part].reshape(g_low.shape).astype(bf16)
+        resid_f = resid_f + matmul(g_low[...], vm.out_proj[part * half_inner : (part + 1) * half_inner])
+    need(loads.shared_gate, loads.shared_up, loads.ffn_gain)
+    resid_f = in_order(resid_f) + h_all[...]
     for place in range(n):
-        part48[place * rows : (place + 1) * rows] = resid_f[8 * place : 8 * place + rows]
+        part48[place * rows : (place + 1) * rows] = resid_f[4 * place : 4 * place + rows]
     resid_part = part48[...].astype(bf16)
     src4[...] = resid_part
     land4[me] = resid_part
-    rows4 = spread(3, src4, land4)
+    rows4 = spread(5, 3, src4, land4)
     gain_part = vm.ffn_gain[:, pl.ds(pl.multiple_of(me * col_width, col_width), col_width)]
     shared_part = (resid_part.astype(f32) * gain_part).astype(bf16)
     slots[:, :shared_units] = matmul(shared_part, vm.shared_gate[...])
     slots[:, shared_units:] = matmul(shared_part, vm.shared_up[...])
     for place in range(n):
         src5[place] = folded(slots[place * rows : (place + 1) * rows], fold5.at[place])
-    scatter(4, src5, land5)
+    scatter(6, src5, land5, whole_sem.at[1])
     land5[me] = src5[me]
 
     need(loads.expert_gate, loads.expert_up, loads.expert_down)
@@ -652,7 +689,7 @@
     acc_up[...] = jnp.zeros_like(acc_up)
     squares = [jnp.zeros((total, col_width), f32)]
 
-    def add_block(owner):
+    def add_block(owner, kind=0):
         piece = land4[owner].astype(f32)
         squares[0] = squares[0] + piece * piece
         at = pl.ds(pl.multiple_of(owner * col_width, col_width), col_width)
@@ -661,15 +698,17 @@
         acc_up[...] += matmul(scaled, vm.expert_up[at])
 
     add_block(me)
-    collect(3, land4, rows4, add_block)
+    finish(collect(5, 3, land4, rows4, add_block), add_block)
     scale_all = lax.rsqrt(jnp.sum(squares[0], axis=1, keepdims=True) / width + epsilon)
     hidden_units = (silu(acc_gate[...] * scale_all) * (acc_up[...] * scale_all)).astype(bf16)
     served = matmul(select, hidden_units).astype(bf16)
-    served_f[...] = matmul(served, vm.expert_down[...])
-    for place in range(n):
-        src6[place] = served_f[2 * place : 2 * place + 2].astype(bf16)
-    scatter(5, src6, land6)
-    land6[me] = src6[me]
+    half_width = width // 2
+    for part in range(2):
+        served_f[...] = matmul(served, vm.expert_down[:, part * half_width : (part + 1) * half_width])
+        for place in range(n):
+            src6[part, place] = served_f[2 * place : 2 * place + 2].astype(bf16)
+        scatter(7 + part, src6.at[part], land6.at[part], part_sem.at[1, me] if part else whole_sem.at[2])
+        land6[part, me] = src6[part, me]
 
     need(loads.router_t, loads.shared_down)
     own_row = lax.broadcasted_iota(jnp.int32, (rows, total), 0) + me * rows
@@ -688,8 +727,8 @@
     middle = weights[1:2]
     inner_w = jnp.concatenate([middle * (1.0 - kept[0:1]), middle * kept[0:1]], axis=0)
     shared = jnp.zeros(fold5.shape[1:], f32)
+    arrived_all(1, land5)
     for place in range(n):
-        arrived(4, src5.at[0], land5, place)
         shared = shared + land5[place].astype(f32)
     wide = shared.shape[1]
     rest = wide // rows
@@ -700,29 +739,38 @@
     shared_hidden = (silu(shared[:, :shared_units]) * shared[:, shared_units:]).astype(bf16)
     start = resid_own + matmul(shared_hidden, vm.shared_down[...])
     y_all[:, :width] = start
-    ends = jnp.zeros((2, width), f32)
-    mid = jnp.zeros((2, width), f32)
-    for place in range(n):
-        arrived(5, src6.at[0], land6, place)
-        piece = land6[place].astype(f32)
-        ends = ends + piece * outer_w[:, place : place + 1]
-        mid = mid + piece * inner_w[:, place : place + 1]
-    xv[0:1, :width] = ends[0:1]
-    xv[1:2, :width] = mid[0:1] + mid[1:2]
-    xv[2:3, :width] = ends[1:2]
+    for part in range(2):
+        ends = jnp.zeros((2, half_width), f32)
+        mid = jnp.zeros((2, half_width), f32)
+        if part == 0:
+            arrived_all(2, land6.at[0])
+        for place in range(n):
+            if part:
+                arrived(1, land6.at[1], place)
+            piece = land6[part, place].astype(f32)
+            ends = ends + piece * outer_w[:, place : place + 1]
+            mid = mid + piece * inner_w[:, place : place + 1]
+        at = slice(part * half_width, (part + 1) * half_width)
+        xv[0:1, at] = ends[0:1]
+        xv[1:2, at] = mid[0:1] + mid[1:2]
+        xv[2:3, at] = ends[1:2]
     layer_out[...] = (y_all[:, :width] + xv[:, :width]).astype(bf16)
-    for one in sent:
-        one.wait_send()
+    for phase, landed in blocks:
+        all_blocks(landed, send_sem.at[phase], whole_sem.at[0]).wait_send()
 
 
 def store_kernel(layer_out, next_state, next_window, layer_hbm, state_hbm, window_hbm, sems):
-    pieces = [(layer_out, layer_hbm), (next_window, window_hbm)]
-    pieces += [(next_state.at[at], state_hbm.at[at]) for at in range(next_state.shape[0])]
-    copies = [pltpu.make_async_copy(a, b, sems.at[at]) for at, (a, b) in enumerate(pieces)]
-    for one in copies:
+    for at in range(next_state.shape[0]):
+        pltpu.make_async_copy(next_state.at[at], state_hbm.at[at], sems.at[0]).start()
+    small = [
+        pltpu.make_async_copy(layer_out, layer_hbm, sems.at[1]),
+        pltpu.make_async_copy(next_window, window_hbm, sems.at[2]),
+    ]
+    for one in small:
         one.start()
-    for one in copies:
+    for one in small:
         one.wait()
+    pltpu.make_async_copy(next_state, state_hbm, sems.at[0]).wait()
 
 
 def one_kernel(*args):
@@ -754,6 +802,7 @@
     named = named._replace(ssm_state=named.ssm_state.reshape(rows * GROUPS, span, STATE))
     conv_dim = named.conv_bias.shape[1]
     cols = 2 * named.gate_proj.shape[1] + 2 * named.write_t.shape[0]
+    gate_cols = named.gate_proj.shape[1]
     col_width = named.out_proj.shape[1]
     shared_units = named.shared_gate.shape[1]
     bf16, f32 = jnp.bfloat16, jnp.float32
@@ -762,26 +811,29 @@
     units = 2 * shared_units
     scratch += [
         V((4, width * 3 // 4), bf16), V((n, 4, width * 3 // 4), bf16),
-        V((n, 4, cols), bf16), V((n, 4, cols), bf16),
-        V((4, inner * 3 // 4), bf16), V((n, 4, inner * 3 // 4), bf16),
+        V((n, 4, cols - gate_cols), bf16), V((n, 4, cols - gate_cols), bf16),
+        V((n, 4, gate_cols), bf16), V((n, 4, gate_cols), bf16),
+        V((2, 4, inner * 3 // 8), bf16), V((2, n, 4, inner * 3 // 8), bf16),
         V((total, col_width), bf16), V((n, total, col_width), bf16),
         V((n, 4, units * 3 // 4), bf16), V((n, 4, units * 3 // 4), bf16),
-        V((n, 2, width), bf16), V((n, 2, width), bf16),
-        V((4, width * 3 // 4), f32), V((4, inner * 3 // 4), f32), V((n, 4, units * 3 // 4), f32),
-        V((n, 8, width), f32), V((n * 8, width), bf16), V((n * 8, cols), f32), V((n, 4, cols), f32),
-        V((n, 8, inner), f32), V((n * 8, inner), bf16), V((n * 8, col_width), f32),
+        V((2, n, 2, width // 2), bf16), V((2, n, 2, width // 2), bf16),
+        V((4, width * 3 // 4), f32), V((4, inner * 3 // 8), f32), V((n, 4, units * 3 // 4), f32),
+        V((n // 2, 8, width), f32), V((n * 4, width), bf16), V((n * 4, cols - gate_cols), f32),
+        V((n * 4, gate_cols), f32), V((n, 4, cols - gate_cols), f32),
+        V((2, n // 2, 8, inner // 2), f32), V((n * 4, inner // 2), bf16), V((n * 4, col_width), f32),
         V((n, 128), f32), V((n, 128), f32), V((total, col_width), f32),
         V((total, shared_units), f32), V((total, shared_units), f32),
         V((rows, conv_dim), f32), V((rows, inner), f32), V((rows, inner), f32), V((rows, conv_dim), f32),
         V((rows, inner), f32), V((GROUPS, rows, STATE), f32), V((GROUPS, rows, STATE), f32),
         V((rows, inner), f32), V((1, inner), f32),
-        V((rows * GROUPS, heads // GROUPS, 128), f32), V((rows * GROUPS, span, STATE), bf16),
-        V((rows, 3, conv_dim), f32), V((total, units), f32), V((2 * n, width), f32),
+        V((rows * GROUPS, heads // GROUPS, 128), f32), V((rows * GROUPS, STATE, span), bf16),
+        V((rows, 3, conv_dim), f32), V((total, units), f32), V((2 * n, width // 2), f32),
+        V((width, cols - 2 * gate_cols), bf16),
         pltpu.SemaphoreType.DMA((len(named),)),
-        pltpu.SemaphoreType.DMA((6, n)),
-        pltpu.SemaphoreType.DMA((6, n)),
-        pltpu.SemaphoreType.DMA((6, n)),
-        pltpu.SemaphoreType.DMA((6, n)),
+        pltpu.SemaphoreType.DMA((9,)),
+        pltpu.SemaphoreType.DMA((4, n)),
+        pltpu.SemaphoreType.DMA((2, n)),
+        pltpu.SemaphoreType.DMA((3,)),
     ]
     layer_out, next_state, next_window = pl.pallas_call(
         functools.partial(layer_kernel, n, rows),
@@ -803,7 +855,7 @@
         out_shape=tuple(jax.ShapeDtypeStruct(one.shape, one.dtype) for one in outs),
         in_specs=[pl.BlockSpec(memory_space=pltpu.VMEM)] * 3,
         out_specs=tuple(pl.BlockSpec(memory_space=pltpu.HBM) for _ in range(3)),
-        scratch_shapes=[pltpu.SemaphoreType.DMA((2 + named.ssm_state.shape[0],))],
+        scratch_shapes=[pltpu.SemaphoreType.DMA((3,))],
         compiler_params=pltpu.CompilerParams(vmem_limit_bytes=1024 * 1024),
     )(*outs)
     return layer_out, next_state.reshape(state_shape), next_window
@@ -817,7 +869,8 @@
         and n & (n - 1) == 0
         and 2 <= n <= 128
         and named.hidden.shape[1] % 512 == 0
-        and 2 * named.gate_proj.shape[1] + 128 == 3 * 128 + 256
+        and named.gate_proj.shape[1] == 256
+        and named.gate_proj.shape[0] * 2 == named.group_gain.shape[0]
         and named.expert_gate.shape[2] == named.shared_gate.shape[1]
         and named.shared_gate.shape[1] % 256 == 0
         and named.hidden.shape[1] <= named.group_gain.shape[0]

time: 44.1 us -> 39.6 us (0.90)
  Pallas kernels: 43.2 us -> 38.7 us
    pallas_call x1, Pallas kernels: 40.3 us -> 36 us  [one_kernel(): pl.pallas_call(functools.partial(layer_kernel, n, rows), out_shape=(pltpu...]
where the time goes in v2:
time: 39.6 us; the launch traced here: 39.4 us
  Pallas kernels  38.7 us (98%)
  between operations  0.65 us (2%)
    pallas_call x1, Pallas kernels, one_kernel(): pl.pallas_call(functools.partial(layer_kernel, n, rows), out_shape=(pltpu...  36 us
    pallas_call x1, Pallas kernels, one_kernel(): pl.pallas_call(store_kernel, out_shape=tuple((jax.ShapeDtypeStruct(one.sh...  2.7 us

profile of v2, /device:TPU:0, one launch (start us, length us, event | category | flops | bytes accessed | tf_op | source)
XLA Modules:
  0.0 39.4 jit_solution(6609257698611949111)
XLA Ops:
  0.6 36.0 %shard_map.265 = (bf16[3,2048]{1,0:T(4,128)(2,1)S(1)}, f32[24,512,128]{2,1,0:T(8,128)S(1)}, bf16[3,3,6144]{2,1,0:T(4,128)(2,1)S(1)}) custom-call(bf16[3,2048]{1,0:T(4,128)(2,1)} %refs_0_.1, bf16[3,3,6144]{2,1,0:T(4,128)(2,1)} %refs_1_.1, f32[24,512,128]{2,1,0:T(8,128)} %bitcast.16, bf16[2048,256]{1,0:T(8,128)(2,1)} %refs_3_.1, bf16[2048,256]{1,0:T(8,128)(2,1)} %refs_4_.1, ...), custom_call_target="tpu_custom_call" | custom-call | tf_op jit(solution)/shard_map/pallas_call | solution.py:838
  36.7 2.7 %shard_map.266 = (bf16[3,2048]{1,0:T(4,128)(2,1)}, f32[24,512,128]{2,1,0:T(8,128)}, bf16[3,3,6144]{2,1,0:T(4,128)(2,1)}) custom-call(bf16[3,2048]{1,0:T(4,128)(2,1)S(1)} %get-tuple-element.9.layer_out, f32[24,512,128]{2,1,0:T(8,128)S(1)} %get-tuple-element.10.next_state, bf16[3,3,6144]{2,1,0:T(4,128)(2,1)S(1)} %get-tuple-element.11.next_window), custom_call_target="tpu_custom_call" | custom-call | tf_op jit(solution)/shard_map/pallas_call | solution.py:853

commit v3 on v2

--- a/solution.py
+++ b/solution.py
@@ -353,38 +353,44 @@
         pl.semaphore_signal(
             barrier, inc=1, device_id={"ep": flipped(step)}, device_id_type=pl.DeviceIdType.MESH
         )
-    loads = Args(
-        *[pltpu.make_async_copy(there, here, in_sem.at[at]) for at, (there, here) in enumerate(zip(hbm, vm))]
-    )
-    for one in (
-        loads.hidden,
-        loads.mix_gain,
-        loads.expert_ids,
-        loads.gate_proj,
-        loads.input_proj,
-        loads.write_t,
-        loads.read_t,
-        loads.step_t,
-        loads.step_bias,
-        loads.decay_log,
-        loads.decay_shift,
-        loads.skip_scale,
-        loads.conv_window,
-        loads.conv_taps,
-        loads.conv_bias,
-        loads.ssm_state,
-        loads.group_gain,
-        loads.out_proj,
-        loads.shared_gate,
-        loads.shared_up,
-        loads.ffn_gain,
-        loads.expert_gate,
-        loads.expert_up,
-        loads.expert_down,
-        loads.router_t,
-        loads.shared_down,
-    ):
+    def load(name, at):
+        return pltpu.make_async_copy(getattr(hbm, name), getattr(vm, name), in_sem.at[at])
+
+    first = (
+        "hidden",
+        "mix_gain",
+        "expert_ids",
+        "write_t",
+        "read_t",
+        "step_t",
+        "step_bias",
+        "decay_log",
+        "decay_shift",
+        "skip_scale",
+        "input_proj",
+        "gate_proj",
+        "conv_window",
+        "conv_taps",
+        "conv_bias",
+        "ssm_state",
+    )
+    later = (
+        "group_gain",
+        "out_proj",
+        "ffn_gain",
+        "shared_gate",
+        "shared_up",
+        "expert_gate",
+        "expert_up",
+        "expert_down",
+        "router_t",
+        "shared_down",
+    )
+    loads = {name: load(name, at) for at, name in enumerate(first)}
+    for one in loads.values():
         one.start()
+    loads.update({name: load(name, at) for at, name in enumerate(later)})
+    loads = Args(**loads)
 
     def need(*these):
         for one in these:
@@ -400,10 +406,15 @@
             device_id_type=pl.DeviceIdType.MESH,
         )
 
-    blocks = []
+    blocks = {}
+
+    def drained(phase):
+        if phase in blocks:
+            all_blocks(blocks.pop(phase), send_sem.at[phase], whole_sem.at[0]).wait_send()
 
     def sends(phase, landed):
-        blocks.append((phase, landed))
+        drained(phase)
+        blocks[phase] = landed
         return send_sem.at[phase]
 
     def all_blocks(landed, sem, arrives):
@@ -414,7 +425,7 @@
         sem = sends(phase, landed)
         out = {}
         for step in range(n - 2, -1, -2):
-            out[step] = remote(source, landed.at[me], sem, ring_sem.at[ring, step + 1], flipped(step + 1))
+            out[step] = remote(source, landed.at[me], sem, ring_sem.at[ring, step], flipped(step + 1))
             out[step].start()
         return out
 
@@ -424,7 +435,7 @@
             out[step].wait_recv()
             owner = flipped(step + 1)
             block = landed.at[owner]
-            one = remote(block, block, send_sem.at[phase], ring_sem.at[ring, step], partner)
+            one = remote(block, block, send_sem.at[phase], ring_sem.at[ring, step - 1], partner)
             one.start()
             passed.append((flipped(step), one))
             take(owner, 0)
@@ -441,11 +452,20 @@
             to = flipped(step)
             remote(source.at[to], landed.at[me], sent, sem, to).start()
 
-    def arrived(part, landed, place):
-        @pl.when(me != place)
+    span_z = min(n, 4)
+
+    def arrived(landed, place):
+        def wait(many):
+            some = landed.at[pl.ds(place, many)]
+            remote(some, some, send_sem.at[0], part_sem.at[place // span_z], partner).wait_recv()
+
+        @pl.when(me // span_z != place // span_z)
         def _():
-            block = landed.at[place]
-            remote(block, block, send_sem.at[0], part_sem.at[part, place], place).wait_recv()
+            wait(span_z)
+
+        @pl.when(me // span_z == place // span_z)
+        def _():
+            wait(span_z - 1)
 
     def arrived_all(which, landed):
         all_blocks(landed, send_sem.at[0], whole_sem.at[which]).wait_recv()
@@ -524,6 +544,8 @@
         window[row, 0:2] = old[1:3]
 
     need(loads.write_t, loads.read_t)
+    for name in later:
+        getattr(loads, name).start()
     vec_proj[...] = jnp.concatenate([vm.write_t[...], vm.read_t[...]], axis=0).T
     unfolded(land1, me, 1, x_all)
     take1 = lambda owner, kind: unfolded(land1, owner, kind, x_all)
@@ -535,7 +557,7 @@
     own_part = lax.broadcasted_iota(jnp.int32, extra.shape[1:], 0) < rows
     for place in range(n):
         src2[place] = jnp.where(own_part, p_all[4 * place : 4 * place + 4], extra[place]).astype(bf16)
-    scatter(1, src2, land2, part_sem.at[0, me])
+    scatter(1, src2, land2, part_sem.at[me // span_z])
     land2[me] = src2[me]
     gate_all[...] = in_order(matmul(x_low[...], vm.gate_proj[...]))
     ends = jnp.concatenate([chosen[0:1], chosen[2:3]], axis=1)
@@ -563,7 +585,8 @@
     for place in range(0, n, 2):
         last = []
         for one in (place, place + 1):
-            arrived(0, land2, one)
+            if one % span_z == 0:
+                arrived(land2, one)
             whole = land2[one].astype(f32)
             piece = whole[0:rows]
             fresh[:, one * gate_cols : (one + 1) * gate_cols] = piece[:, :gate_cols]
@@ -605,7 +628,7 @@
         packed = folded(y_all[:, part * half_inner : (part + 1) * half_inner], fold3)
         src3[part] = packed
         land3[part, me] = packed
-        return spread(3 + part, 1 + part, src3.at[part], land3.at[part])
+        return spread(3 + part, part, src3.at[part], land3.at[part])
 
     half_inner = inner // 2
     for group in range(groups // 2):
@@ -660,7 +683,7 @@
     passed3 = []
     for part in range(2):
         take3[part](me, 1)
-        passed3.append(collect(3 + part, 1 + part, land3.at[part], rows3[part], take3[part]))
+        passed3.append(collect(3 + part, part, land3.at[part], rows3[part], take3[part]))
     need(loads.out_proj)
     resid_f = jnp.zeros(h_all.shape, f32)
     for part in range(2):
@@ -674,14 +697,14 @@
     resid_part = part48[...].astype(bf16)
     src4[...] = resid_part
     land4[me] = resid_part
-    rows4 = spread(5, 3, src4, land4)
+    rows4 = spread(0, 2, src4, land4)
     gain_part = vm.ffn_gain[:, pl.ds(pl.multiple_of(me * col_width, col_width), col_width)]
     shared_part = (resid_part.astype(f32) * gain_part).astype(bf16)
     slots[:, :shared_units] = matmul(shared_part, vm.shared_gate[...])
     slots[:, shared_units:] = matmul(shared_part, vm.shared_up[...])
     for place in range(n):
         src5[place] = folded(slots[place * rows : (place + 1) * rows], fold5.at[place])
-    scatter(6, src5, land5, whole_sem.at[1])
+    scatter(1, src5, land5, whole_sem.at[0])
     land5[me] = src5[me]
 
     need(loads.expert_gate, loads.expert_up, loads.expert_down)
@@ -698,7 +721,7 @@
         acc_up[...] += matmul(scaled, vm.expert_up[at])
 
     add_block(me)
-    finish(collect(5, 3, land4, rows4, add_block), add_block)
+    finish(collect(0, 2, land4, rows4, add_block), add_block)
     scale_all = lax.rsqrt(jnp.sum(squares[0], axis=1, keepdims=True) / width + epsilon)
     hidden_units = (silu(acc_gate[...] * scale_all) * (acc_up[...] * scale_all)).astype(bf16)
     served = matmul(select, hidden_units).astype(bf16)
@@ -707,7 +730,7 @@
         served_f[...] = matmul(served, vm.expert_down[:, part * half_width : (part + 1) * half_width])
         for place in range(n):
             src6[part, place] = served_f[2 * place : 2 * place + 2].astype(bf16)
-        scatter(7 + part, src6.at[part], land6.at[part], part_sem.at[1, me] if part else whole_sem.at[2])
+        scatter(2 + part, src6.at[part], land6.at[part], part_sem.at[me // span_z] if part else whole_sem.at[1])
         land6[part, me] = src6[part, me]
 
     need(loads.router_t, loads.shared_down)
@@ -727,7 +750,7 @@
     middle = weights[1:2]
     inner_w = jnp.concatenate([middle * (1.0 - kept[0:1]), middle * kept[0:1]], axis=0)
     shared = jnp.zeros(fold5.shape[1:], f32)
-    arrived_all(1, land5)
+    arrived_all(0, land5)
     for place in range(n):
         shared = shared + land5[place].astype(f32)
     wide = shared.shape[1]
@@ -743,10 +766,10 @@
         ends = jnp.zeros((2, half_width), f32)
         mid = jnp.zeros((2, half_width), f32)
         if part == 0:
-            arrived_all(2, land6.at[0])
+            arrived_all(1, land6.at[0])
         for place in range(n):
-            if part:
-                arrived(1, land6.at[1], place)
+            if part and place % span_z == 0:
+                arrived(land6.at[1], place)
             piece = land6[part, place].astype(f32)
             ends = ends + piece * outer_w[:, place : place + 1]
             mid = mid + piece * inner_w[:, place : place + 1]
@@ -755,8 +778,8 @@
         xv[1:2, at] = mid[0:1] + mid[1:2]
         xv[2:3, at] = ends[1:2]
     layer_out[...] = (y_all[:, :width] + xv[:, :width]).astype(bf16)
-    for phase, landed in blocks:
-        all_blocks(landed, send_sem.at[phase], whole_sem.at[0]).wait_send()
+    for phase in tuple(blocks):
+        drained(phase)
 
 
 def store_kernel(layer_out, next_state, next_window, layer_hbm, state_hbm, window_hbm, sems):
@@ -829,11 +852,11 @@
         V((rows * GROUPS, heads // GROUPS, 128), f32), V((rows * GROUPS, STATE, span), bf16),
         V((rows, 3, conv_dim), f32), V((total, units), f32), V((2 * n, width // 2), f32),
         V((width, cols - 2 * gate_cols), bf16),
-        pltpu.SemaphoreType.DMA((len(named),)),
-        pltpu.SemaphoreType.DMA((9,)),
-        pltpu.SemaphoreType.DMA((4, n)),
-        pltpu.SemaphoreType.DMA((2, n)),
-        pltpu.SemaphoreType.DMA((3,)),
+        pltpu.SemaphoreType.DMA((16,)),
+        pltpu.SemaphoreType.DMA((5,)),
+        pltpu.SemaphoreType.DMA((3, n - 1)),
+        pltpu.SemaphoreType.DMA((max(1, n // 4),)),
+        pltpu.SemaphoreType.DMA((2,)),
     ]
     layer_out, next_state, next_window = pl.pallas_call(
         functools.partial(layer_kernel, n, rows),

time: 39.6 us -> 38.4 us (0.970)
  Pallas kernels: 38.7 us -> 37.5 us
    pallas_call x1, Pallas kernels: 36 us -> 34.8 us  [one_kernel(): pl.pallas_call(functools.partial(layer_kernel, n, rows), out_shape=(pltpu...]
where the time goes in v3:
time: 38.4 us; the launch traced here: 38.1 us
  Pallas kernels  37.5 us (98%)
  between operations  0.65 us (2%)
    pallas_call x1, Pallas kernels, one_kernel(): pl.pallas_call(functools.partial(layer_kernel, n, rows), out_shape=(pltpu...  34.8 us
    pallas_call x1, Pallas kernels, one_kernel(): pl.pallas_call(store_kernel, out_shape=tuple((jax.ShapeDtypeStruct(one.sh...  2.7 us

profile of v3, /device:TPU:0, one launch (start us, length us, event | category | flops | bytes accessed | tf_op | source)
XLA Modules:
  0.0 38.1 jit_solution(11875401613887479878)
XLA Ops:
  0.6 34.8 %shard_map.265 = (bf16[3,2048]{1,0:T(4,128)(2,1)S(1)}, f32[24,512,128]{2,1,0:T(8,128)S(1)}, bf16[3,3,6144]{2,1,0:T(4,128)(2,1)S(1)}) custom-call(bf16[3,2048]{1,0:T(4,128)(2,1)} %refs_0_.1, bf16[3,3,6144]{2,1,0:T(4,128)(2,1)} %refs_1_.1, f32[24,512,128]{2,1,0:T(8,128)} %bitcast.16, bf16[2048,256]{1,0:T(8,128)(2,1)} %refs_3_.1, bf16[2048,256]{1,0:T(8,128)(2,1)} %refs_4_.1, ...), custom_call_target="tpu_custom_call" | custom-call | tf_op jit(solution)/shard_map/pallas_call | solution.py:861
  35.4 2.7 %shard_map.266 = (bf16[3,2048]{1,0:T(4,128)(2,1)}, f32[24,512,128]{2,1,0:T(8,128)}, bf16[3,3,6144]{2,1,0:T(4,128)(2,1)}) custom-call(bf16[3,2048]{1,0:T(4,128)(2,1)S(1)} %get-tuple-element.9.layer_out, f32[24,512,128]{2,1,0:T(8,128)S(1)} %get-tuple-element.10.next_state, bf16[3,3,6144]{2,1,0:T(4,128)(2,1)S(1)} %get-tuple-element.11.next_window), custom_call_target="tpu_custom_call" | custom-call | tf_op jit(solution)/shard_map/pallas_call | solution.py:876

commit v4 on v3

--- a/solution.py
+++ b/solution.py
@@ -315,10 +315,10 @@
     vm = Args(*refs[count + 3 : 2 * count + 3])
     (
         src1, land1, src2, land2, src_g, land_g, src3, land3, src4, land4, src5, land5, src6, land6,
-        fold1, fold3, fold5, x_all, x_low, p_all, gate_all, extra, g_all, g_low, h_all, flag0, flag2, part48,
+        fold1, fold3, fold5, x_all, x_low, p_all, gate_all, g_all, g_low, h_all, flag0, flag2, part48,
         acc_gate, acc_up, base, cols, y_all, fresh, xv, wv, rv, step_x, skip_x,
         decay_col, decayed, window, slots, served_f, vec_proj,
-        in_sem, send_sem, ring_sem, part_sem, whole_sem,
+        src_h, land_h, mate_proj, mate_gate, mate_up, in_sem, send_sem, ring_sem, part_sem, whole_sem, mate_sem,
     ) = refs[2 * count + 3 :]
     me = lax.axis_index("ep")
     f32, bf16 = jnp.float32, jnp.bfloat16
@@ -410,15 +410,16 @@
 
     def drained(phase):
         if phase in blocks:
-            all_blocks(blocks.pop(phase), send_sem.at[phase], whole_sem.at[0]).wait_send()
-
-    def sends(phase, landed):
+            landed, count = blocks.pop(phase)
+            all_blocks(landed, send_sem.at[phase], whole_sem.at[0], count).wait_send()
+
+    def sends(phase, landed, count=n - 1):
         drained(phase)
-        blocks[phase] = landed
+        blocks[phase] = (landed, count)
         return send_sem.at[phase]
 
-    def all_blocks(landed, sem, arrives):
-        many = landed.at[pl.ds(0, n - 1)]
+    def all_blocks(landed, sem, arrives, count=n - 1):
+        many = landed.at[pl.ds(0, count)]
         return remote(many, many, sem, arrives, partner)
 
     def spread(phase, ring, source, landed):
@@ -428,6 +429,12 @@
             out[step] = remote(source, landed.at[me], sem, ring_sem.at[ring, step], flipped(step + 1))
             out[step].start()
         return out
+
+    def across(phase, source_of, target_ref, landed, sem_of):
+        sem = sends(phase, landed, n // 2)
+        for step in range(n - 1, 0, -2):
+            to = flipped(step)
+            remote(source_of(to), target_ref, sem, sem_of(step), to).start()
 
     def collect(phase, ring, landed, out, take):
         passed = [(partner, out[0])]
@@ -467,8 +474,8 @@
         def _():
             wait(span_z - 1)
 
-    def arrived_all(which, landed):
-        all_blocks(landed, send_sem.at[0], whole_sem.at[which]).wait_recv()
+    def arrived_all(which, landed, count=n - 1):
+        all_blocks(landed, send_sem.at[0], whole_sem.at[which], count).wait_recv()
 
     def folded(value, buffer):
         wide = buffer.shape[1]
@@ -503,17 +510,24 @@
     land1[me] = packed
     pl.semaphore_wait(barrier, n - 1)
     rows1 = spread(0, 0, src1, land1)
+    mates = [
+        remote(there, here, mate_sem.at[2 * at], mate_sem.at[2 * at + 1], partner)
+        for at, (there, here) in enumerate(
+            ((hbm.out_proj, mate_proj), (hbm.shared_gate, mate_gate), (hbm.shared_up, mate_up))
+        )
+    ]
+    for one in mates:
+        one.start()
 
     lane = lax.broadcasted_iota(jnp.int32, (rows, 128), 1)
     ids = vm.expert_ids[...]
     chosen = jnp.zeros((rows, 128), f32)
     for k in range(ids.shape[1]):
         chosen = jnp.where(lane == ids[:, k : k + 1], 1.0, chosen)
-    for place in range(n):
-        for row in range(rows):
-            extra[place, rows : rows + 1, row * col_width : (row + 1) * col_width] = own[
-                row : row + 1, place * col_width : (place + 1) * col_width
-            ]
+    duo = 2 * col_width
+    core = lax.rem(me, 2)
+    for chip in range(n // 2):
+        src_h[chip] = vm.hidden[:, chip * duo : (chip + 1) * duo]
     need(loads.step_t, loads.step_bias, loads.decay_log, loads.decay_shift, loads.skip_scale)
     raw = dot_t(normed, vm.step_t[...]) + vm.step_bias[...]
     step_size = jnp.maximum(raw, 0.0) + jnp.log1p(jnp.exp(-jnp.abs(raw)))
@@ -554,9 +568,8 @@
     x_low[...] = x_all[...].reshape(x_low.shape).astype(bf16)
     p_all[:, :gate_cols] = in_order(matmul(x_low[...], vm.input_proj[...]))
     p_all[:, gate_cols:] = in_order(matmul(x_low[...], vec_proj[...]))
-    own_part = lax.broadcasted_iota(jnp.int32, extra.shape[1:], 0) < rows
     for place in range(n):
-        src2[place] = jnp.where(own_part, p_all[4 * place : 4 * place + 4], extra[place]).astype(bf16)
+        src2[place] = p_all[4 * place : 4 * place + 4].astype(bf16)
     scatter(1, src2, land2, part_sem.at[me // span_z])
     land2[me] = src2[me]
     gate_all[...] = in_order(matmul(x_low[...], vm.gate_proj[...]))
@@ -567,6 +580,7 @@
         src_g[place] = jnp.where(own_part, gate_all[4 * place : 4 * place + 4], ends).astype(bf16)
     scatter(2, src_g, land_g, whole_sem.at[0])
     land_g[me] = src_g[me]
+    across(4, lambda to: src_h.at[to // 2], land_h.at[me // 2], land_h, lambda step: whole_sem.at[2])
 
     need(loads.ssm_state)
 
@@ -591,10 +605,6 @@
             piece = whole[0:rows]
             fresh[:, one * gate_cols : (one + 1) * gate_cols] = piece[:, :gate_cols]
             last.append(piece[:, gate_cols:])
-            for row in range(rows):
-                h_all[4 * one + row : 4 * one + row + 1] = whole[
-                    rows : rows + 1, row * col_width : (row + 1) * col_width
-                ]
         low = lax.broadcasted_iota(jnp.int32, last[0].shape, 1) < half
         at = slice(inner + place * half, inner + (place + 2) * half)
         fresh[:, at] = jnp.where(low, last[0], pltpu.roll(last[1], half, 1))
@@ -627,8 +637,13 @@
     def share(part):
         packed = folded(y_all[:, part * half_inner : (part + 1) * half_inner], fold3)
         src3[part] = packed
-        land3[part, me] = packed
-        return spread(3 + part, part, src3.at[part], land3.at[part])
+        across(
+            5 + part,
+            lambda to: src3.at[part],
+            land3.at[part, me // 2],
+            land3.at[part],
+            lambda step: ring_sem.at[part, step - 1],
+        )
 
     half_inner = inner // 2
     for group in range(groups // 2):
@@ -642,11 +657,11 @@
         flag2[place : place + 1] = whole[rows : rows + 1, 128:]
     for group in range(groups // 2):
         gated(group)
-    rows3 = [share(0)]
+    share(0)
     for group in range(groups // 2, groups):
         mix(group)
         gated(group)
-    rows3.append(share(1))
+    share(1)
 
     for group in range(groups):
         at = slice(group * span, (group + 1) * span)
@@ -665,7 +680,8 @@
 
     slot_row = lax.broadcasted_iota(jnp.int32, (2 * n, total), 0)
     slot_lane = lax.broadcasted_iota(jnp.int32, (2 * n, total), 1)
-    first_row = (slot_row // 2) * rows
+    half_rows = total // 2
+    first_row = (slot_row // 2) % 2 * half_rows + slot_row // 4 * rows
     even = slot_row % 2 == 0
     outer = jnp.where(even, first_row, first_row + 2)
     whose = lax.broadcasted_iota(jnp.int32, (2 * n, n), 1) == lax.broadcasted_iota(jnp.int32, (2 * n, n), 0) // 2
@@ -679,49 +695,69 @@
     source_row = jnp.where(flag > 0.5, outer, first_row + 1)
     select = jnp.where(slot_lane == source_row, 1.0, 0.0).astype(bf16)
 
-    take3 = [lambda owner, kind, part=part: unfolded(land3.at[part], owner, kind, g_all.at[part]) for part in range(2)]
-    passed3 = []
+    arrived_all(2, land_h, n // 2)
+    for chip in range(n // 2):
+        h_all[chip * rows : (chip + 1) * rows] = land_h[chip].astype(f32)
+    need(loads.out_proj)
+    mates[0].wait_recv()
+    resid_f = [jnp.zeros((n * 4, col_width), f32)] * 2
     for part in range(2):
-        take3[part](me, 1)
-        passed3.append(collect(3 + part, part, land3.at[part], rows3[part], take3[part]))
-    need(loads.out_proj)
-    resid_f = jnp.zeros(h_all.shape, f32)
-    for part in range(2):
-        finish(passed3[part], take3[part])
+        for step in range(1, n, 2):
+            chip = flipped(step) // 2
+            block = land3.at[part, chip]
+            remote(block, block, send_sem.at[0], ring_sem.at[part, step - 1], partner).wait_recv()
+            piece = block[...].astype(f32)
+            wide = piece.shape[1]
+            rest = wide // rows
+            g_all[part, chip, 0:rows, :wide] = piece[0:rows]
+            for row in range(rows):
+                g_all[part, chip, row : row + 1, wide:] = piece[rows : rows + 1, row * rest : (row + 1) * rest]
         g_low[...] = g_all[part].reshape(g_low.shape).astype(bf16)
-        resid_f = resid_f + matmul(g_low[...], vm.out_proj[part * half_inner : (part + 1) * half_inner])
+        at = slice(part * half_inner, (part + 1) * half_inner)
+        resid_f = [
+            resid_f[0] + matmul(g_low[...], vm.out_proj[at]),
+            resid_f[1] + matmul(g_low[...], mate_proj[at]),
+        ]
     need(loads.shared_gate, loads.shared_up, loads.ffn_gain)
-    resid_f = in_order(resid_f) + h_all[...]
-    for place in range(n):
-        part48[place * rows : (place + 1) * rows] = resid_f[4 * place : 4 * place + rows]
-    resid_part = part48[...].astype(bf16)
+    for which, place in enumerate((core, 1 - core)):
+        for chip in range(n // 2):
+            part48[which, chip * rows : (chip + 1) * rows] = resid_f[which][8 * chip : 8 * chip + rows]
+    swap = lambda left, right: jnp.where(core == 0, jnp.concatenate([left, right], axis=1), jnp.concatenate([right, left], axis=1))
+    resid_part = (swap(part48[0], part48[1]) + h_all[...]).astype(bf16)
     src4[...] = resid_part
     land4[me] = resid_part
     rows4 = spread(0, 2, src4, land4)
-    gain_part = vm.ffn_gain[:, pl.ds(pl.multiple_of(me * col_width, col_width), col_width)]
+    gain_part = vm.ffn_gain[:, pl.ds(pl.multiple_of(me // 2 * duo, duo), duo)]
     shared_part = (resid_part.astype(f32) * gain_part).astype(bf16)
-    slots[:, :shared_units] = matmul(shared_part, vm.shared_gate[...])
-    slots[:, shared_units:] = matmul(shared_part, vm.shared_up[...])
-    for place in range(n):
-        src5[place] = folded(slots[place * rows : (place + 1) * rows], fold5.at[place])
-    scatter(1, src5, land5, whole_sem.at[0])
-    land5[me] = src5[me]
+    mates[1].wait_recv()
+    mates[2].wait_recv()
+    lower, upper = shared_part[:, :col_width], shared_part[:, col_width:]
+    mine = jnp.where(core == 0, lower.astype(f32), upper.astype(f32)).astype(bf16)
+    other = jnp.where(core == 0, upper.astype(f32), lower.astype(f32)).astype(bf16)
+    slots[:, :shared_units] = matmul(mine, vm.shared_gate[...]) + matmul(other, mate_gate[...])
+    slots[:, shared_units:] = matmul(mine, vm.shared_up[...]) + matmul(other, mate_up[...])
+    for chip in range(n // 2):
+        src5[chip] = folded(slots[chip * rows : (chip + 1) * rows], fold5.at[chip])
+    across(1, lambda to: src5.at[to // 2], land5.at[me // 2], land5, lambda step: whole_sem.at[0])
 
     need(loads.expert_gate, loads.expert_up, loads.expert_down)
     acc_gate[...] = jnp.zeros_like(acc_gate)
     acc_up[...] = jnp.zeros_like(acc_up)
-    squares = [jnp.zeros((total, col_width), f32)]
-
-    def add_block(owner, kind=0):
-        piece = land4[owner].astype(f32)
+    squares = [jnp.zeros((total, duo), f32)]
+
+    def chip_rows(chip):
+        return jnp.concatenate([land4[2 * chip + 1].astype(f32), land4[2 * chip].astype(f32)], axis=0)
+
+    def add_chip(owner, kind):
+        chip = owner // 2
+        piece = chip_rows(chip)
         squares[0] = squares[0] + piece * piece
-        at = pl.ds(pl.multiple_of(owner * col_width, col_width), col_width)
+        at = pl.ds(pl.multiple_of(chip * duo, duo), duo)
         scaled = (piece * vm.ffn_gain[:, at]).astype(bf16)
         acc_gate[...] += matmul(scaled, vm.expert_gate[at])
         acc_up[...] += matmul(scaled, vm.expert_up[at])
 
-    add_block(me)
-    finish(collect(0, 2, land4, rows4, add_block), add_block)
+    finish(collect(0, 2, land4, rows4, lambda owner, kind: None), add_chip)
     scale_all = lax.rsqrt(jnp.sum(squares[0], axis=1, keepdims=True) / width + epsilon)
     hidden_units = (silu(acc_gate[...] * scale_all) * (acc_up[...] * scale_all)).astype(bf16)
     served = matmul(select, hidden_units).astype(bf16)
@@ -734,11 +770,10 @@
         land6[part, me] = src6[part, me]
 
     need(loads.router_t, loads.shared_down)
-    own_row = lax.broadcasted_iota(jnp.int32, (rows, total), 0) + me * rows
+    own_row = lax.broadcasted_iota(jnp.int32, (rows, total), 0) + core * half_rows + me // 2 * rows
     pick = jnp.where(lax.broadcasted_iota(jnp.int32, (rows, total), 1) == own_row, 1.0, 0.0).astype(bf16)
-    for place in range(n):
-        at = slice(place * col_width, (place + 1) * col_width)
-        y_all[:, at] = matmul(pick, land4[place])
+    for chip in range(n // 2):
+        y_all[:, chip * duo : (chip + 1) * duo] = matmul(pick, chip_rows(chip).astype(bf16))
     resid_own = y_all[:, :width]
     norm_scale = lax.rsqrt(jnp.mean(resid_own * resid_own, axis=-1, keepdims=True) + epsilon)
     routed_own = (resid_own * norm_scale * vm.ffn_gain[...]).astype(bf16)
@@ -750,9 +785,9 @@
     middle = weights[1:2]
     inner_w = jnp.concatenate([middle * (1.0 - kept[0:1]), middle * kept[0:1]], axis=0)
     shared = jnp.zeros(fold5.shape[1:], f32)
-    arrived_all(0, land5)
-    for place in range(n):
-        shared = shared + land5[place].astype(f32)
+    arrived_all(0, land5, n // 2)
+    for chip in range(n // 2):
+        shared = shared + land5[chip].astype(f32)
     wide = shared.shape[1]
     rest = wide // rows
     cols[:, :wide] = shared[0:rows]
@@ -780,6 +815,8 @@
     layer_out[...] = (y_all[:, :width] + xv[:, :width]).astype(bf16)
     for phase in tuple(blocks):
         drained(phase)
+    for one in mates:
+        one.wait_send()
 
 
 def store_kernel(layer_out, next_state, next_window, layer_hbm, state_hbm, window_hbm, sems):
@@ -836,27 +873,30 @@
         V((4, width * 3 // 4), bf16), V((n, 4, width * 3 // 4), bf16),
         V((n, 4, cols - gate_cols), bf16), V((n, 4, cols - gate_cols), bf16),
         V((n, 4, gate_cols), bf16), V((n, 4, gate_cols), bf16),
-        V((2, 4, inner * 3 // 8), bf16), V((2, n, 4, inner * 3 // 8), bf16),
-        V((total, col_width), bf16), V((n, total, col_width), bf16),
-        V((n, 4, units * 3 // 4), bf16), V((n, 4, units * 3 // 4), bf16),
+        V((2, 4, inner * 3 // 8), bf16), V((2, n // 2, 4, inner * 3 // 8), bf16),
+        V((total // 2, 2 * col_width), bf16), V((n, total // 2, 2 * col_width), bf16),
+        V((n // 2, 4, units * 3 // 4), bf16), V((n // 2, 4, units * 3 // 4), bf16),
         V((2, n, 2, width // 2), bf16), V((2, n, 2, width // 2), bf16),
-        V((4, width * 3 // 4), f32), V((4, inner * 3 // 8), f32), V((n, 4, units * 3 // 4), f32),
+        V((4, width * 3 // 4), f32), V((4, inner * 3 // 8), f32), V((n // 2, 4, units * 3 // 4), f32),
         V((n // 2, 8, width), f32), V((n * 4, width), bf16), V((n * 4, cols - gate_cols), f32),
-        V((n * 4, gate_cols), f32), V((n, 4, cols - gate_cols), f32),
-        V((2, n // 2, 8, inner // 2), f32), V((n * 4, inner // 2), bf16), V((n * 4, col_width), f32),
-        V((n, 128), f32), V((n, 128), f32), V((total, col_width), f32),
+        V((n * 4, gate_cols), f32),
+        V((2, n // 2, 8, inner // 2), f32), V((n * 4, inner // 2), bf16), V((total // 2, 2 * col_width), f32),
+        V((n, 128), f32), V((n, 128), f32), V((2, total // 2, col_width), f32),
         V((total, shared_units), f32), V((total, shared_units), f32),
         V((rows, conv_dim), f32), V((rows, inner), f32), V((rows, inner), f32), V((rows, conv_dim), f32),
         V((rows, inner), f32), V((GROUPS, rows, STATE), f32), V((GROUPS, rows, STATE), f32),
         V((rows, inner), f32), V((1, inner), f32),
         V((rows * GROUPS, heads // GROUPS, 128), f32), V((rows * GROUPS, STATE, span), bf16),
-        V((rows, 3, conv_dim), f32), V((total, units), f32), V((2 * n, width // 2), f32),
+        V((rows, 3, conv_dim), f32), V((total // 2, units), f32), V((2 * n, width // 2), f32),
         V((width, cols - 2 * gate_cols), bf16),
+        V((n // 2, rows, 2 * col_width), bf16), V((n // 2, rows, 2 * col_width), bf16),
+        V(named.out_proj.shape, bf16), V(named.shared_gate.shape, bf16), V(named.shared_up.shape, bf16),
         pltpu.SemaphoreType.DMA((16,)),
-        pltpu.SemaphoreType.DMA((5,)),
+        pltpu.SemaphoreType.DMA((7,)),
         pltpu.SemaphoreType.DMA((3, n - 1)),
         pltpu.SemaphoreType.DMA((max(1, n // 4),)),
-        pltpu.SemaphoreType.DMA((2,)),
+        pltpu.SemaphoreType.DMA((3,)),
+        pltpu.SemaphoreType.DMA((6,)),
     ]
     layer_out, next_state, next_window = pl.pallas_call(
         functools.partial(layer_kernel, n, rows),

time: 38.4 us -> 37.9 us (0.987)
  Pallas kernels: 37.5 us -> 37 us
    pallas_call x1, Pallas kernels: 34.8 us -> 34.3 us  [one_kernel(): pl.pallas_call(functools.partial(layer_kernel, n, rows), out_shape=(pltpu...]
where the time goes in v4:
time: 37.9 us; the launch traced here: 37.7 us
  Pallas kernels  37 us (98%)
  between operations  0.65 us (2%)
    pallas_call x1, Pallas kernels, one_kernel(): pl.pallas_call(functools.partial(layer_kernel, n, rows), out_shape=(pltpu...  34.3 us
    pallas_call x1, Pallas kernels, one_kernel(): pl.pallas_call(store_kernel, out_shape=tuple((jax.ShapeDtypeStruct(one.sh...  2.7 us

profile of v4, /device:TPU:0, one launch (start us, length us, event | category | flops | bytes accessed | tf_op | source)
XLA Modules:
  0.0 37.7 jit_solution(13880597523587959729)
XLA Ops:
  0.6 34.3 %shard_map.265 = (bf16[3,2048]{1,0:T(4,128)(2,1)S(1)}, f32[24,512,128]{2,1,0:T(8,128)S(1)}, bf16[3,3,6144]{2,1,0:T(4,128)(2,1)S(1)}) custom-call(bf16[3,2048]{1,0:T(4,128)(2,1)} %refs_0_.1, bf16[3,3,6144]{2,1,0:T(4,128)(2,1)} %refs_1_.1, f32[24,512,128]{2,1,0:T(8,128)} %bitcast.16, bf16[2048,256]{1,0:T(8,128)(2,1)} %refs_3_.1, bf16[2048,256]{1,0:T(8,128)(2,1)} %refs_4_.1, ...), custom_call_target="tpu_custom_call" | custom-call | tf_op jit(solution)/shard_map/pallas_call | solution.py:901
  35.0 2.7 %shard_map.266 = (bf16[3,2048]{1,0:T(4,128)(2,1)}, f32[24,512,128]{2,1,0:T(8,128)}, bf16[3,3,6144]{2,1,0:T(4,128)(2,1)}) custom-call(bf16[3,2048]{1,0:T(4,128)(2,1)S(1)} %get-tuple-element.9.layer_out, f32[24,512,128]{2,1,0:T(8,128)S(1)} %get-tuple-element.10.next_state, bf16[3,3,6144]{2,1,0:T(4,128)(2,1)S(1)} %get-tuple-element.11.next_window), custom_call_target="tpu_custom_call" | custom-call | tf_op jit(solution)/shard_map/pallas_call | solution.py:916

commit v5 on v4

--- a/solution.py
+++ b/solution.py
@@ -318,7 +318,7 @@
         fold1, fold3, fold5, x_all, x_low, p_all, gate_all, g_all, g_low, h_all, flag0, flag2, part48,
         acc_gate, acc_up, base, cols, y_all, fresh, xv, wv, rv, step_x, skip_x,
         decay_col, decayed, window, slots, served_f, vec_proj,
-        src_h, land_h, mate_proj, mate_gate, mate_up, in_sem, send_sem, ring_sem, part_sem, whole_sem, mate_sem,
+        src_h, land_h, mate_proj, mate_gate, mate_up, in_sem, send_sem, ring_sem, part_sem, whole_sem, mate_sem, half_sem, by_chip,
     ) = refs[2 * count + 3 :]
     me = lax.axis_index("ep")
     f32, bf16 = jnp.float32, jnp.bfloat16
@@ -642,7 +642,7 @@
             lambda to: src3.at[part],
             land3.at[part, me // 2],
             land3.at[part],
-            lambda step: ring_sem.at[part, step - 1],
+            lambda step: half_sem.at[step // 2] if part else ring_sem.at[0, step - 1],
         )
 
     half_inner = inner // 2
@@ -700,18 +700,20 @@
         h_all[chip * rows : (chip + 1) * rows] = land_h[chip].astype(f32)
     need(loads.out_proj)
     mates[0].wait_recv()
-    resid_f = [jnp.zeros((n * 4, col_width), f32)] * 2
+    resid_f = [jnp.zeros((n * 2, col_width), f32)] * 2
     for part in range(2):
         for step in range(1, n, 2):
             chip = flipped(step) // 2
             block = land3.at[part, chip]
-            remote(block, block, send_sem.at[0], ring_sem.at[part, step - 1], partner).wait_recv()
+            sem = half_sem.at[step // 2] if part else ring_sem.at[0, step - 1]
+            remote(block, block, send_sem.at[0], sem, partner).wait_recv()
             piece = block[...].astype(f32)
             wide = piece.shape[1]
             rest = wide // rows
-            g_all[part, chip, 0:rows, :wide] = piece[0:rows]
+            tile, low = step // 4, 4 * (step // 2 % 2)
+            g_all[part, tile, low : low + rows, :wide] = piece[0:rows]
             for row in range(rows):
-                g_all[part, chip, row : row + 1, wide:] = piece[rows : rows + 1, row * rest : (row + 1) * rest]
+                g_all[part, tile, low + row : low + row + 1, wide:] = piece[rows : rows + 1, row * rest : (row + 1) * rest]
         g_low[...] = g_all[part].reshape(g_low.shape).astype(bf16)
         at = slice(part * half_inner, (part + 1) * half_inner)
         resid_f = [
@@ -720,13 +722,15 @@
         ]
     need(loads.shared_gate, loads.shared_up, loads.ffn_gain)
     for which, place in enumerate((core, 1 - core)):
+        for step in range(1, n, 2):
+            by_chip[which, flipped(step) // 2] = resid_f[which][2 * step - 2 : 2 * step + 2]
         for chip in range(n // 2):
-            part48[which, chip * rows : (chip + 1) * rows] = resid_f[which][8 * chip : 8 * chip + rows]
+            part48[which, chip * rows : (chip + 1) * rows] = by_chip[which, chip, 0:rows]
     swap = lambda left, right: jnp.where(core == 0, jnp.concatenate([left, right], axis=1), jnp.concatenate([right, left], axis=1))
     resid_part = (swap(part48[0], part48[1]) + h_all[...]).astype(bf16)
     src4[...] = resid_part
     land4[me] = resid_part
-    rows4 = spread(0, 2, src4, land4)
+    rows4 = spread(0, 1, src4, land4)
     gain_part = vm.ffn_gain[:, pl.ds(pl.multiple_of(me // 2 * duo, duo), duo)]
     shared_part = (resid_part.astype(f32) * gain_part).astype(bf16)
     mates[1].wait_recv()
@@ -757,7 +761,7 @@
         acc_gate[...] += matmul(scaled, vm.expert_gate[at])
         acc_up[...] += matmul(scaled, vm.expert_up[at])
 
-    finish(collect(0, 2, land4, rows4, lambda owner, kind: None), add_chip)
+    finish(collect(0, 1, land4, rows4, lambda owner, kind: None), add_chip)
     scale_all = lax.rsqrt(jnp.sum(squares[0], axis=1, keepdims=True) / width + epsilon)
     hidden_units = (silu(acc_gate[...] * scale_all) * (acc_up[...] * scale_all)).astype(bf16)
     served = matmul(select, hidden_units).astype(bf16)
@@ -880,7 +884,7 @@
         V((4, width * 3 // 4), f32), V((4, inner * 3 // 8), f32), V((n // 2, 4, units * 3 // 4), f32),
         V((n // 2, 8, width), f32), V((n * 4, width), bf16), V((n * 4, cols - gate_cols), f32),
         V((n * 4, gate_cols), f32),
-        V((2, n // 2, 8, inner // 2), f32), V((n * 4, inner // 2), bf16), V((total // 2, 2 * col_width), f32),
+        V((2, n // 4, 8, inner // 2), f32), V((n * 2, inner // 2), bf16), V((total // 2, 2 * col_width), f32),
         V((n, 128), f32), V((n, 128), f32), V((2, total // 2, col_width), f32),
         V((total, shared_units), f32), V((total, shared_units), f32),
         V((rows, conv_dim), f32), V((rows, inner), f32), V((rows, inner), f32), V((rows, conv_dim), f32),
@@ -893,10 +897,12 @@
         V(named.out_proj.shape, bf16), V(named.shared_gate.shape, bf16), V(named.shared_up.shape, bf16),
         pltpu.SemaphoreType.DMA((16,)),
         pltpu.SemaphoreType.DMA((7,)),
-        pltpu.SemaphoreType.DMA((3, n - 1)),
+        pltpu.SemaphoreType.DMA((2, n - 1)),
         pltpu.SemaphoreType.DMA((max(1, n // 4),)),
         pltpu.SemaphoreType.DMA((3,)),
         pltpu.SemaphoreType.DMA((6,)),
+        pltpu.SemaphoreType.DMA((n // 2,)),
+        V((2, n // 2, 4, col_width), f32),
     ]
     layer_out, next_state, next_window = pl.pallas_call(
         functools.partial(layer_kernel, n, rows),

time: 37.9 us -> 37.9 us (level)
  no operation moved by 1% of the time
where the time goes in v5:
time: 37.9 us; the launch traced here: 37.6 us
  Pallas kernels  37 us (98%)
  between operations  0.65 us (2%)
    pallas_call x1, Pallas kernels, one_kernel(): pl.pallas_call(functools.partial(layer_kernel, n, rows), out_shape=(pltpu...  34.3 us
    pallas_call x1, Pallas kernels, one_kernel(): pl.pallas_call(store_kernel, out_shape=tuple((jax.ShapeDtypeStruct(one.sh...  2.7 us

profile of v5, /device:TPU:0, one launch (start us, length us, event | category | flops | bytes accessed | tf_op | source)
XLA Modules:
  0.0 37.6 jit_solution(1637782659736953485)
XLA Ops:
  0.6 34.3 %shard_map.265 = (bf16[3,2048]{1,0:T(4,128)(2,1)S(1)}, f32[24,512,128]{2,1,0:T(8,128)S(1)}, bf16[3,3,6144]{2,1,0:T(4,128)(2,1)S(1)}) custom-call(bf16[3,2048]{1,0:T(4,128)(2,1)} %refs_0_.1, bf16[3,3,6144]{2,1,0:T(4,128)(2,1)} %refs_1_.1, f32[24,512,128]{2,1,0:T(8,128)} %bitcast.16, bf16[2048,256]{1,0:T(8,128)(2,1)} %refs_3_.1, bf16[2048,256]{1,0:T(8,128)(2,1)} %refs_4_.1, ...), custom_call_target="tpu_custom_call" | custom-call | tf_op jit(solution)/shard_map/pallas_call | solution.py:907
  34.9 2.7 %shard_map.266 = (bf16[3,2048]{1,0:T(4,128)(2,1)}, f32[24,512,128]{2,1,0:T(8,128)}, bf16[3,3,6144]{2,1,0:T(4,128)(2,1)}) custom-call(bf16[3,2048]{1,0:T(4,128)(2,1)S(1)} %get-tuple-element.9.layer_out, f32[24,512,128]{2,1,0:T(8,128)S(1)} %get-tuple-element.10.next_state, bf16[3,3,6144]{2,1,0:T(4,128)(2,1)S(1)} %get-tuple-element.11.next_window), custom_call_target="tpu_custom_call" | custom-call | tf_op jit(solution)/shard_map/pallas_call | solution.py:922
